TPU v7x, 32 devices: a whole 2x2x4 slice. The times are simulated.
32 devices in a mesh: fs: 16 (over z, y, x), tp: 2 (over core).
Axes of the slice: x: 2, y: 2, z: 4, core: 2. Of those that a mesh axis runs over, the one named last changes fastest.
Arguments:
- normed: bfloat16 [16384, 2048], P('fs'), may hold values from -6 to 6
- key_cot: bfloat16 [16384, 1024], P('fs', 'tp'), may hold values from -130 to 130
- value_cot: bfloat16 [16384, 2048], P('fs', 'tp'), may hold values from -130 to 130
- basis: bfloat16 [2048, 256], P('fs'), may hold values from -3.535534 to 3.535534
- master_key: float32 [2048, 1024], P('fs', 'tp'), may hold values from -3 to 3
- master_value: float32 [2048, 2048], P('fs', 'tp'), may hold values from -3 to 3
- first_key: float32 [256, 1024], P('fs', 'tp'), may hold values from -3 to 3
- second_key: float32 [256, 1024], P('fs', 'tp'), may hold values from 0.05 to 2
- first_value: float32 [256, 2048], P('fs', 'tp'), may hold values from -3 to 3
- second_value: float32 [256, 2048], P('fs', 'tp'), may hold values from 0.05 to 2
Outputs:
- step_key: float32 [2048, 1024], P('fs', 'tp')
- step_value: float32 [2048, 2048], P('fs', 'tp')
- new_master_key: float32 [2048, 1024], P('fs', 'tp')
- new_master_value: float32 [2048, 2048], P('fs', 'tp')
- copy_key: bfloat16 [2048, 1024], P(None, 'tp')
- copy_value: bfloat16 [2048, 2048], P(None, 'tp')
- new_first_key: float32 [256, 1024], P('fs', 'tp')
- new_second_key: float32 [256, 1024], P('fs', 'tp')
- new_first_value: float32 [256, 2048], P('fs', 'tp')
- new_second_value: float32 [256, 2048], P('fs', 'tp')
All inputs are finite; a program needn't handle non-finite values.
Results may differ from a plain program's by a relative error of at most 0.0055.
Values may be sent and summed in bfloat16 or wider, within the bound.
No kernel may reach another device: no remote copies, remote signals or barrier semaphores. Data moves between devices by JAX's collectives and lax.ppermute only.
A program may use at most 64 MiB of HBM per device.

v0:
```python
import jax
import jax.numpy as jnp
from jax import lax
from jax.sharding import PartitionSpec as P

DK = 1024
DV = 2048
R = 256


learn_rate = 0.05
beta_first = 0.9
beta_second = 0.9
epsilon = 1e-08
norm_eps = 1e-06


def on_device(
    normed,
    key_cot,
    value_cot,
    basis,
    master_key,
    master_value,
    first_key,
    second_key,
    first_value,
    second_value,
):
    key_cols = key_cot.shape[1]
    cotangents = jnp.concatenate([key_cot, value_cot], axis=1)
    projected = jnp.dot(
        normed, lax.all_gather(basis, "fs", axis=0, tiled=True), preferred_element_type=jnp.float32
    )
    upper_part = projected.astype(jnp.bfloat16)
    lower_part = (projected - upper_part.astype(jnp.float32)).astype(jnp.bfloat16)
    partial_value = lax.dot_general(
        upper_part, cotangents, (((0,), (0,)), ((), ())), preferred_element_type=jnp.float32
    )
    partial_value = partial_value + lax.dot_general(
        lower_part, cotangents, (((0,), (0,)), ((), ())), preferred_element_type=jnp.float32
    )
    rank_rows = first_key.shape[0]
    summed = lax.psum(partial_value, "fs")
    squares = lax.psum(jnp.sum(summed * summed), "tp")
    own_rows = lax.dynamic_slice_in_dim(summed, lax.axis_index("fs") * rank_rows, rank_rows, 0)
    root_mean = jnp.sqrt(squares / (R * (DK + DV)) + norm_eps)
    grad_scale = 1.0 / root_mean
    first_moment = jnp.concatenate([first_key, first_value], axis=1)
    second_moment = jnp.concatenate([second_key, second_value], axis=1)
    scaled = own_rows * grad_scale
    new_first = beta_first * first_moment + (1.0 - beta_first) * scaled
    new_second = beta_second * second_moment + (1.0 - beta_second) * scaled * scaled
    direction = (new_first / (jnp.sqrt(new_second) + epsilon)).astype(jnp.bfloat16)
    all_directions = lax.all_gather(direction, "fs", axis=0, tiled=True)
    update_step = jnp.dot(basis, all_directions, preferred_element_type=jnp.float32)
    master = jnp.concatenate([master_key, master_value], axis=1)
    new_master = master - learn_rate * update_step
    half_copy = new_master.astype(jnp.bfloat16)
    copy_key, copy_value = (
        lax.all_gather(half_copy[:, :key_cols], "fs", axis=0, tiled=True),
        lax.all_gather(half_copy[:, key_cols:], "fs", axis=0, tiled=True),
    )
    return (
        update_step[:, :key_cols],
        update_step[:, key_cols:],
        new_master[:, :key_cols],
        new_master[:, key_cols:],
        copy_key,
        copy_value,
        new_first[:, :key_cols],
        new_second[:, :key_cols],
        new_first[:, key_cols:],
        new_second[:, key_cols:],
    )


def solution(mesh):
    placed = (
        P("fs", None),
        P("fs", "tp"),
        P("fs", "tp"),
        P("fs", None),
        P("fs", "tp"),
        P("fs", "tp"),
        P("fs", "tp"),
        P("fs", "tp"),
        P("fs", "tp"),
        P("fs", "tp"),
    )
    return jax.shard_map(
        on_device,
        mesh=mesh,
        in_specs=placed,
        out_specs=(
            P("fs", "tp"),
            P("fs", "tp"),
            P("fs", "tp"),
            P("fs", "tp"),
            P(None, "tp"),
            P(None, "tp"),
            P("fs", "tp"),
            P("fs", "tp"),
            P("fs", "tp"),
            P("fs", "tp"),
        ),
        check_vma=False,
    )
```

profile of v0, /device:TPU:0, one launch (start us, length us, event | category | flops | bytes accessed | tf_op | source)
XLA Modules:
  0.0 406.0 jit_solution(744935510458757411)
XLA Ops:
  7.2 0.0 all-gather.4.cloned.1.call-start
  7.2 0.7 all-gather.4.cloned.1.call-update
  7.9 0.0 all-reduce.2.cloned.1.call-start
  8.0 0.0 copy-start
  8.0 1.4 constant_dynamic-update-slice_fusion.1
  9.4 0.5 copy-done
  9.9 0.2 constant_dynamic-update-slice_fusion
  10.0 58.5 %all-gather.4.cloned.1.call-done = bf16[2048,256]{1,0:T(8,128)(2,1)} async-done(((bf16[128,256]{1,0:T(8,128)(2,1)}), bf16[2048,256]{1,0:T(8,128)(2,1)}) %all-gather.4.cloned.1.call-update) | async-done | bytes 1048592 | tf_op jit(solution)/shard_map/all_gather | solution.py:33
  68.6 3.7 fusion.6
  72.3 1.0 fusion.1
  73.4 0.0 copy-start.2
  73.4 2.2 convolution_add_fusion
  75.5 0.0 copy-start.3
  75.5 0.0 copy-start.4
  75.5 0.0 copy-start.5
  75.5 0.0 copy-start.6
  75.5 0.0 copy-start.1
  75.6 0.0 all-reduce.2.cloned.1.call-update
  75.6 0.0 all-gather.6.cloned.1.call-start
  75.6 0.0 copy-done.2
  75.7 0.1 copy.20
  75.8 1.2 copy.21
  77.0 115.1 %all-reduce.2.cloned.1.call-done = f32[256,1536]{1,0:T(8,128)} async-done(((f32[256,1536]{1,0:T(8,128)}), f32[256,1536]{1,0:T(8,128)}) %all-reduce.2.cloned.1.call-update) | async-done | bytes 1572880 | tf_op jit(solution)/shard_map/psum | solution.py:44
  192.1 2.4 multiply_reduce_fusion
  194.5 3.1 psum.15
  198.3 0.0 copy-done.3
  198.3 0.0 copy-done.4
  198.3 0.0 copy-done.5
  198.3 0.0 copy-done.6
  198.3 1.0 divide_convert_fusion
  199.3 43.7 %all_gather.13 = bf16[256,1536]{1,0:T(8,128)(2,1)S(1)} all-gather(bf16[16,1536]{1,0:T(8,128)(2,1)S(1)} %get-tuple-element.22), channel_id=1, replica_groups=mesh['fs'=16,'tp'=2] {'fs'}, dimensions={0}, use_global_device_ids=true | all-gather | bytes 835584 | tf_op jit(solution)/shard_map/all_gather | solution.py:55
  243.0 0.0 copy-done.1
  243.0 0.4 fusion.4
  243.4 0.7 slice.44
  244.1 0.0 all-gather.6.cloned.1.call-update
  244.1 0.0 all-gather.8.cloned.1.call-start
  244.1 0.7 slice.45
  244.9 0.0 all-gather.8.cloned.1.call-update
  244.9 0.6 slice.47
  245.5 0.6 slice.49
  246.1 0.6 slice.46
  246.7 0.6 slice.48
  247.5 1.0 copy.25
  248.5 0.8 copy.24
  249.4 1.0 copy.23
  250.3 0.8 copy.22
  251.2 51.9 %all-gather.6.cloned.1.call-done = bf16[2048,512]{0,1:T(8,128)(2,1)} async-done(((bf16[128,512]{0,1:T(8,128)(2,1)}), bf16[2048,512]{0,1:T(8,128)(2,1)}) %all-gather.6.cloned.1.call-update) | async-done | bytes 2097168 | tf_op jit(solution)/shard_map/all_gather | solution.py:61
  303.0 3.9 copy.26
  307.0 86.1 %all-gather.8.cloned.1.call-done = bf16[2048,1024]{0,1:T(8,128)(2,1)} async-done(((bf16[128,1024]{0,1:T(8,128)(2,1)}), bf16[2048,1024]{0,1:T(8,128)(2,1)}) %all-gather.8.cloned.1.call-update) | async-done | bytes 4194320 | tf_op jit(solution)/shard_map/all_gather | solution.py:62
  393.1 6.4 %copy.27 = bf16[2048,1024]{1,0:T(8,128)(2,1)} copy(bf16[2048,1024]{0,1:T(8,128)(2,1)} %all-gather.8.cloned.1.call-done) | data formatting | bytes 8388608
  (4 shorter events, 0.1 us)
Async XLA Ops:
  7.2 61.4 %all-gather.4.cloned.1.call-start = ((), (), s32[]{:S(2)}) async-start(), calls=%async_computation | async-start | bytes 1114112 | tf_op jit(solution)/shard_map/all_gather | solution.py:33
  7.9 184.2 %all-reduce.2.cloned.1.call-start = ((), (), s32[]{:S(2)}) async-start(), calls=%async_computation.1 | async-start | bytes 3145728 | tf_op jit(solution)/shard_map/psum | solution.py:44
  8.0 1.9 copy-start
  73.4 2.3 copy-start.2
  75.5 122.7 %copy-start.3 = (f32[16,1024]{1,0:T(8,128)S(1)}, f32[16,1024]{1,0:T(8,128)}, u32[]{:S(2)}) copy-start(f32[16,1024]{1,0:T(8,128)} %param.19) | copy-start | bytes 196612
  75.5 122.8 %copy-start.4 = (f32[16,1024]{1,0:T(8,128)S(1)}, f32[16,1024]{1,0:T(8,128)}, u32[]{:S(2)}) copy-start(f32[16,1024]{1,0:T(8,128)} %param.18) | copy-start | bytes 196612
  75.5 122.8 %copy-start.5 = (f32[16,512]{1,0:T(8,128)S(1)}, f32[16,512]{1,0:T(8,128)}, u32[]{:S(2)}) copy-start(f32[16,512]{1,0:T(8,128)} %param.17) | copy-start | bytes 98308
  75.5 122.8 %copy-start.6 = (f32[16,512]{1,0:T(8,128)S(1)}, f32[16,512]{1,0:T(8,128)}, u32[]{:S(2)}) copy-start(f32[16,512]{1,0:T(8,128)} %param.16) | copy-start | bytes 98308
  75.5 167.4 %copy-start.1 = (bf16[128,256]{1,0:T(8,128)(2,1)S(1)}, bf16[128,256]{1,0:T(8,128)(2,1)}, u32[]{:S(2)}) copy-start(bf16[128,256]{1,0:T(8,128)(2,1)} %param.13) | copy-start | bytes 196612
  75.6 227.5 %all-gather.6.cloned.1.call-start = ((), (), s32[]{:S(2)}) async-start(), calls=%async_computation.2 | async-start | bytes 2228224 | tf_op jit(solution)/shard_map/all_gather | solution.py:61
  244.1 149.0 %all-gather.8.cloned.1.call-start = ((), (), s32[]{:S(2)}) async-start(), calls=%async_computation.3 | async-start | bytes 4456448 | tf_op jit(solution)/shard_map/all_gather | solution.py:62
Sparse Core Ops, SparseCore 0:
  10.7 57.7 all-gather.3
  75.7 116.3 all-reduce.1
  244.2 58.7 all-gather.5
  306.2 86.8 all-gather.7
where the time goes:
time: 406 us
  waiting for transfers between devices  312 us (77%)
  blocking collectives  46.8 us (12%)
  local copies, waits for them, and re-layouts  21.4 us (5%)
  between operations  14.6 us (4%)
  matrix products  7.34 us (2%)
    psum x1, waiting for transfers between devices, on_device(): summed = lax.psum(partial_value, 'fs')  115 us
    all_gather x1, waiting for transfers between devices, on_device(): lax.all_gather(half_copy[:, key_cols:], 'fs', axis=0, tiled=True)  86.1 us
    all_gather x1, waiting for transfers between devices, on_device(): lax.all_gather(basis, 'fs', axis=0, tiled=True)  58.5 us
    all_gather x1, waiting for transfers between devices, on_device(): lax.all_gather(half_copy[:, :key_cols], 'fs', axis=0, tiled=True)  51.9 us
    all_gather x1, blocking collectives, on_device(): all_directions = lax.all_gather(direction, 'fs', axis=0, tiled=True)  43.7 us
    unnamed x23, local copies, waits for them, and re-layouts  17.3 us
  transfers between devices with their start and end apart: 4, of which 4 were waited for; matrix products, arithmetic and copies ran while one was open for 3% of the time, Pallas kernels for 0%

commit v1 on v0

v1 whole, which is shorter than its diff:
```python
import functools

import jax
import jax.numpy as jnp
from jax import lax
from jax.experimental import pallas as pl
from jax.experimental.pallas import tpu as pltpu
from jax.sharding import PartitionSpec as P


learn_rate = 0.05
beta_first = 0.9
beta_second = 0.9
epsilon = 1e-08
norm_eps = 1e-06

INNER = 4


def swap(values, ranks, offset):
    return lax.ppermute(values, "fs", [(rank, rank ^ offset) for rank in range(ranks)])


def place(pieces, me, ranks, rows):
    whole = jnp.zeros((ranks * rows, pieces[0].shape[1]), pieces[0].dtype)
    for inner, column in enumerate(pieces):
        for outer in range(ranks // INNER):
            whole = lax.dynamic_update_slice_in_dim(
                whole, column[outer * rows : (outer + 1) * rows], (me ^ (outer * INNER + inner)) * rows, 0
            )
    return whole


def outer_column(block, ranks):
    pieces = [block] + [swap(block, ranks, INNER * step) for step in range(1, ranks // INNER)]
    return jnp.concatenate(pieces, axis=0)


def inner_gather(column, me, ranks, rows):
    column = lax.optimization_barrier(column)
    pieces = [column] + [swap(column, ranks, step) for step in range(1, INNER)]
    return place(pieces, me, ranks, rows)


def spread(block, ranks):
    last = ranks // INNER - 1
    chunks = []
    for chunk in range(last + 1):
        if chunk == last and chunk > 1:
            shard = swap(chunks[chunk - 1][1][0][2], ranks, INNER)
        else:
            shard = swap(block, ranks, INNER * chunk) if chunk else block
        first = swap(shard, ranks, 1)
        second = swap(shard, ranks, 2)
        if chunk == last:
            third = swap(shard, ranks, 3)
        elif chunk % 2:
            third = swap(first, ranks, 2)
        else:
            third = swap(second, ranks, 1)
        chunks.append((chunk, [(away, 0, part) for away, part in enumerate((shard, first, second, third))]))
    return chunks


def prepare_kernel(master_key, master_value, first_key, second_key, first_value, second_value, master, moments):
    key_cols = master_key.shape[1]
    cols = master.shape[1]
    master[:, :key_cols] = master_key[...].astype(jnp.bfloat16)
    master[:, key_cols:] = master_value[...].astype(jnp.bfloat16)
    moments[:, :key_cols] = first_key[...].astype(jnp.bfloat16)
    moments[:, key_cols:cols] = first_value[...].astype(jnp.bfloat16)
    moments[:, cols : cols + key_cols] = second_key[...].astype(jnp.bfloat16)
    moments[:, cols + key_cols :] = second_value[...].astype(jnp.bfloat16)


def prepare(master_key, master_value, first_key, second_key, first_value, second_value):
    cols = master_key.shape[1] + master_value.shape[1]
    return pl.pallas_call(
        prepare_kernel,
        out_shape=[
            jax.ShapeDtypeStruct((master_key.shape[0], cols), jnp.bfloat16),
            jax.ShapeDtypeStruct((first_key.shape[0], 2 * cols), jnp.bfloat16),
        ],
        name="prepare",
    )(master_key, master_value, first_key, second_key, first_value, second_value)


def gather_basis(basis, ranks):
    half = basis.shape[1] // 2
    others = lax.axis_size("tp")
    core = lax.axis_index("tp") % 2
    own = lax.dynamic_slice_in_dim(basis, core * half, half, 1)
    column = outer_column(own, ranks)
    mine = [column] + [swap(column, ranks, step) for step in range(1, INNER)]
    theirs = []
    for piece in mine:
        theirs.append(lax.ppermute(piece, "tp", [(rank, rank ^ 1) for rank in range(others)]))
    return mine, theirs


PARTS = 2


def project_kernel(groups, where, *refs):
    mine, theirs, refs = refs[:INNER], refs[INNER : 2 * INNER], refs[2 * INNER :]
    normed, key_cot, value_cot, whole_out, home, *aways = refs[: 5 + INNER - 1]
    tokens, cots, upper, whole, partial, home_buf, away_buf, token_sem, cot_sem, give_sem = refs[5 + INNER - 1 :]
    height = tokens.shape[0] // PARTS
    key_cols = key_cot.shape[1]
    loads = [
        pltpu.make_async_copy(
            normed.at[pl.ds(part * height, height)], tokens.at[pl.ds(part * height, height)], token_sem.at[part]
        )
        for part in range(PARTS)
    ]
    for load in loads:
        load.start()
    cot_loads = [
        pltpu.make_async_copy(key_cot, cots.at[:, pl.ds(0, key_cols)], cot_sem.at[0]),
        pltpu.make_async_copy(value_cot, cots.at[:, pl.ds(key_cols, value_cot.shape[1])], cot_sem.at[1]),
    ]
    for load in cot_loads:
        load.start()
    me, core = where[0], where[1]
    half = mine[0].shape[1]
    rows = mine[0].shape[0] // groups
    for first in range(2):

        @pl.when(core == first)
        def _(first=first):
            for away in range(INNER):
                for group in range(groups):
                    spot = pl.ds(pl.multiple_of((me ^ (group * INNER + away)) * rows, rows), rows)
                    part = slice(group * rows, (group + 1) * rows)
                    whole[spot, first * half : (first + 1) * half] = mine[away][part, :]
                    whole[spot, (1 - first) * half : (2 - first) * half] = theirs[away][part, :]

    gives = [pltpu.make_async_copy(whole, whole_out, give_sem.at[INNER])]
    gives[0].start()
    for part in range(PARTS):
        loads[part].wait()
        span = slice(part * height, (part + 1) * height)
        upper[span, :] = jnp.dot(tokens[span, :], whole[...], preferred_element_type=jnp.float32).astype(jnp.bfloat16)
    for load in cot_loads:
        load.wait()
    partial[...] = lax.dot_general(
        upper[...], cots[...], (((0,), (0,)), ((), ())), preferred_element_type=jnp.float32
    )
    if len(home.shape) == 2:
        gives.append(pltpu.make_async_copy(partial, home, give_sem.at[0]))
        gives[-1].start()
    else:
        low_rows = home.shape[1]
        for away in reversed(range(INNER)):
            for group in range(home.shape[0]):
                slot = group * INNER + ((me % INNER) ^ away)
                block = partial[pl.ds(pl.multiple_of(slot * low_rows, low_rows), low_rows), :]
                if away:
                    away_buf[away - 1, group] = block.astype(jnp.bfloat16)
                else:
                    home_buf[group] = block
            source, target = (away_buf.at[away - 1], aways[away - 1]) if away else (home_buf, home)
            gives.append(pltpu.make_async_copy(source, target, give_sem.at[away]))
            gives[-1].start()
    for give in gives:
        give.wait()


def project(mine, theirs, normed, key_cot, value_cot, me, ranks):
    depth = 2 * mine[0].shape[1]
    groups = ranks // INNER
    low_rows = depth // ranks
    cols = key_cot.shape[1] + value_cot.shape[1]
    where = jnp.stack([me, lax.axis_index("tp") % 2]).astype(jnp.int32)
    local = pl.BlockSpec(memory_space=pltpu.VMEM)
    anywhere = pl.BlockSpec(memory_space=pl.ANY)
    tidy = low_rows % 8 == 0
    home = jax.ShapeDtypeStruct((groups, low_rows, cols) if tidy else (depth, cols), jnp.float32)
    away = jax.ShapeDtypeStruct((groups, low_rows, cols) if tidy else (8, 128), jnp.bfloat16)
    whole, home, *aways = pl.pallas_call(
        functools.partial(project_kernel, groups),
        in_specs=[pl.BlockSpec(memory_space=pltpu.SMEM)] + [local] * (2 * INNER) + [anywhere] * 3,
        out_specs=[anywhere] * 2 + [anywhere if tidy else local] * (INNER - 1),
        out_shape=[jax.ShapeDtypeStruct((normed.shape[1], depth), jnp.bfloat16), home] + [away] * (INNER - 1),
        scratch_shapes=[
            pltpu.VMEM(normed.shape, jnp.bfloat16),
            pltpu.VMEM((normed.shape[0], cols), jnp.bfloat16),
            pltpu.VMEM((normed.shape[0], depth), jnp.bfloat16),
            pltpu.VMEM((normed.shape[1], depth), jnp.bfloat16),
            pltpu.VMEM((depth, cols), jnp.float32),
            pltpu.VMEM((groups, low_rows, cols), jnp.float32),
            pltpu.VMEM((INNER - 1, groups, low_rows, cols), jnp.bfloat16),
            pltpu.SemaphoreType.DMA((PARTS,)),
            pltpu.SemaphoreType.DMA((2,)),
            pltpu.SemaphoreType.DMA((INNER + 1,)),
        ],
        name="project",
    )(where, *mine, *theirs, normed, key_cot, value_cot)
    if not tidy:
        blocks = home.reshape(groups, INNER, low_rows, cols)
        inner = me % INNER
        home = lax.dynamic_index_in_dim(blocks, inner, 1, keepdims=False)
        aways = [
            lax.dynamic_index_in_dim(blocks, inner ^ step, 1, keepdims=False).astype(jnp.bfloat16)
            for step in range(1, INNER)
        ]
    return whole, home, aways


def scatter_sum(total, aways, me, ranks):
    groups = ranks // INNER
    for step, away in enumerate(aways, 1):
        total = total + swap(away, ranks, step).astype(jnp.float32)
    high = me // INNER
    own = lax.dynamic_index_in_dim(total, high, 0, keepdims=False)
    for step in range(1, groups):
        away = lax.dynamic_index_in_dim(total, high ^ step, 0, keepdims=False).astype(jnp.bfloat16)
        own = own + swap(away, ranks, step * INNER).astype(jnp.float32)
    return own


def pair_sum(parts):
    while len(parts) > 1:
        parts = [left + right for left, right in zip(parts[::2], parts[1::2])]
    return parts[0]


def sum_everywhere(rows_of, ranks):
    value = pair_sum([jnp.sum((part * part).reshape(part.shape[0], -1, 128), axis=1) for part in rows_of])
    received = [swap(value, ranks, step) for step in range(1, INNER)]
    value = pair_sum([value] + received)
    others = lax.axis_size("tp")
    total = value
    for step in range(1, others):
        total = total + lax.ppermute(value, "tp", [(rank, (rank + step) % others) for rank in range(others)])
    return jnp.sum(total)


def copy_kernel(layout, with_own, inherited, *refs):
    count = sum(len(parts) for _, parts in layout)
    order, basis, directions, *rest = refs
    pieces, rest = rest[:count], rest[count:]
    masters, rest = (rest[:2], rest[2:]) if with_own else ((), rest)
    rest = rest[inherited:]
    copy_key, copy_value, *rest = rest
    results, rest = (rest[:4], rest[4:]) if with_own else ((), rest)
    taken, made, step, take_sem, key_sem, value_sem, *rest = rest
    rows = step.shape[0] // INNER
    key_cols = copy_key.shape[1]
    here = order[0]
    inner = here % INNER
    outer = here // INNER
    takes = [
        pltpu.make_async_copy(piece, taken.at[slot, pl.ds(0, piece.shape[0])], take_sem.at[slot])
        for slot, piece in enumerate(pieces)
    ]
    for take in takes:
        take.start()
    if with_own:
        own_key, own_value, own_step, own_take, own_give = rest
        own_takes = [
            pltpu.make_async_copy(masters[0], own_key, own_take.at[0]),
            pltpu.make_async_copy(masters[1], own_value, own_take.at[1]),
        ]
        for take in own_takes:
            take.start()
    gives = []
    slot = 0
    for chunk, parts in layout:
        first_row = pl.multiple_of((outer ^ chunk) * INNER * rows, INNER * rows)
        if len(parts) == INNER:
            step[...] = jnp.dot(
                basis[pl.ds(first_row, INNER * rows), :], directions[...], preferred_element_type=jnp.float32
            )
        for away, start in parts:
            size = pieces[slot].shape[0]
            spot = pl.multiple_of((inner ^ away) * rows + start, size)
            if len(parts) != INNER:
                step[pl.ds(spot, size), :] = jnp.dot(
                    basis[pl.ds(pl.multiple_of(first_row + spot, size), size), :],
                    directions[...],
                    preferred_element_type=jnp.float32,
                )
            takes[slot].wait()
            change = learn_rate * step[pl.ds(spot, size), :]
            made[slot, pl.ds(0, size)] = (taken[slot, pl.ds(0, size)].astype(jnp.float32) - change).astype(jnp.bfloat16)
            target = pl.ds(pl.multiple_of(first_row + spot, size), size)
            for out_ref, columns, sem in (
                (copy_key, pl.ds(0, key_cols), key_sem),
                (copy_value, pl.ds(key_cols, step.shape[1] - key_cols), value_sem),
            ):
                give = pltpu.make_async_copy(
                    made.at[slot, pl.ds(0, size), columns], out_ref.at[target, :], sem.at[slot]
                )
                give.start()
                gives.append(give)
            slot += 1
        if with_own and chunk == 0:
            for take in own_takes:
                take.wait()
            own_step[...] = step[pl.ds(pl.multiple_of(inner * rows, rows), rows), :]
            own_key[...] = own_key[...] - learn_rate * own_step[:, :key_cols]
            own_value[...] = own_value[...] - learn_rate * own_step[:, key_cols:]
            value_cols = step.shape[1] - key_cols
            for place_in, (source, target) in enumerate(
                (
                    (own_step.at[:, pl.ds(0, key_cols)], results[0]),
                    (own_step.at[:, pl.ds(key_cols, value_cols)], results[1]),
                    (own_key, results[2]),
                    (own_value, results[3]),
                )
            ):
                give = pltpu.make_async_copy(source, target, own_give.at[place_in])
                give.start()
                gives.append(give)
    for give in gives:
        give.wait()


def write_copies(chunks, masters, me, basis, directions, key_cols, ranks, earlier):
    rows = basis.shape[0] // ranks
    cols = directions.shape[1]
    layout = tuple((chunk, tuple((away, start) for away, start, _ in parts)) for chunk, parts in chunks)
    pieces = [part for _, parts in chunks for _, _, part in parts]
    count = len(pieces)
    tallest = max(piece.shape[0] for piece in pieces)
    anywhere = pl.BlockSpec(memory_space=pl.ANY)
    local = pl.BlockSpec(memory_space=pltpu.VMEM)
    out_shape = [
        jax.ShapeDtypeStruct((ranks * rows, key_cols), jnp.bfloat16),
        jax.ShapeDtypeStruct((ranks * rows, cols - key_cols), jnp.bfloat16),
    ]
    scratch = [
        pltpu.VMEM((count, tallest, cols), jnp.bfloat16),
        pltpu.VMEM((count, tallest, cols), jnp.bfloat16),
        pltpu.VMEM((INNER * rows, cols), jnp.float32),
        pltpu.SemaphoreType.DMA((count,)),
        pltpu.SemaphoreType.DMA((count,)),
        pltpu.SemaphoreType.DMA((count,)),
    ]
    if masters:
        out_shape += [jax.ShapeDtypeStruct(master.shape, jnp.float32) for master in (*masters, *masters)]
        scratch += [
            pltpu.VMEM(masters[0].shape, jnp.float32),
            pltpu.VMEM(masters[1].shape, jnp.float32),
            pltpu.VMEM((rows, cols), jnp.float32),
            pltpu.SemaphoreType.DMA((2,)),
            pltpu.SemaphoreType.DMA((4,)),
        ]
    first_alias = 3 + count + len(masters)
    return pl.pallas_call(
        functools.partial(copy_kernel, layout, bool(masters), len(earlier)),
        in_specs=[pl.BlockSpec(memory_space=pltpu.SMEM), local, local]
        + [anywhere] * (count + len(masters) + len(earlier)),
        out_specs=[anywhere] * len(out_shape),
        out_shape=out_shape,
        scratch_shapes=scratch,
        input_output_aliases={first_alias: 0, first_alias + 1: 1} if earlier else {},
    )(me.reshape(1), basis, directions, *pieces, *masters, *earlier)


def on_device(
    total_count,
    ranks,
    normed,
    key_cot,
    value_cot,
    basis,
    master_key,
    master_value,
    first_key,
    second_key,
    first_value,
    second_value,
):
    me = lax.axis_index("fs")
    key_cols = key_cot.shape[1]
    mine, theirs = gather_basis(basis, ranks)
    master, moments_sent = prepare(master_key, master_value, first_key, second_key, first_value, second_value)
    chunks = spread(master, ranks)
    moments = outer_column(moments_sent, ranks).astype(jnp.float32)
    whole_basis, home, aways = project(mine, theirs, normed, key_cot, value_cot, me, ranks)
    low = scatter_sum(home, aways, me, ranks)
    low_column = outer_column(low.astype(jnp.bfloat16), ranks).astype(jnp.float32)
    height = low.shape[0]
    squares = sum_everywhere(
        [low_column[start : start + height] for start in range(0, low_column.shape[0], height)], ranks
    )
    grad_scale = 1.0 / jnp.sqrt(squares / total_count + norm_eps)

    def advance(low_part, first, second):
        scaled = low_part * grad_scale
        new_first = beta_first * first + (1.0 - beta_first) * scaled
        new_second = beta_second * second + (1.0 - beta_second) * scaled * scaled
        return new_first, new_second

    cols = low.shape[1]
    new_first, new_second = advance(low_column, moments[:, :cols], moments[:, cols:])
    direction = (new_first / (jnp.sqrt(new_second) + epsilon)).astype(jnp.bfloat16)
    directions = inner_gather(direction, me, ranks, low.shape[0])
    first_key, second_key, first_value, second_value, low = lax.optimization_barrier(
        (first_key, second_key, first_value, second_value, low)
    )
    new_first_key, new_second_key = advance(low[:, :key_cols], first_key, second_key)
    new_first_value, new_second_value = advance(low[:, key_cols:], first_value, second_value)
    copy_key, copy_value, *own = write_copies(
        chunks[:-1], (master_key, master_value), me, whole_basis, directions, key_cols, ranks, ()
    )
    copy_key, copy_value = write_copies(
        chunks[-1:], (), me, whole_basis, directions, key_cols, ranks, (copy_key, copy_value)
    )
    return (*own, copy_key, copy_value, new_first_key, new_second_key, new_first_value, new_second_value)


def solution(mesh):
    split = P("fs", "tp")
    rows = P("fs", None)
    ranks = mesh.shape["fs"]
    tensor = mesh.shape["tp"]

    def body(*arguments):
        first_key, first_value = arguments[6], arguments[8]
        count = ranks * tensor * (first_key.size + first_value.size)
        return on_device(count, ranks, *arguments)

    return jax.shard_map(
        body,
        mesh=mesh,
        in_specs=(rows, split, split, rows) + (split,) * 6,
        out_specs=(split,) * 4 + (P(None, "tp"),) * 2 + (split,) * 4,
        check_vma=False,
    )
```

time: 406 us -> 170 us (0.42)
  waiting for transfers between devices: 312 us -> 89.2 us
  starting transfers between devices: 0.16 us -> 47 us
  blocking collectives: 46.8 us -> 0 us
  Pallas kernels: 0 us -> 21.6 us
  local copies, waits for them, and re-layouts: 21.4 us -> 5.1 us
  between operations: 14.6 us -> 1.86 us
  matrix products: 7.34 us -> 0 us
    all_gather x3 -> x0, waiting for transfers between devices: 197 us -> none  [the longest x1 86.1 us: on_device(): lax.all_gather(half_copy[:, key_cols:], 'fs', axis=0, tiled=True)]
    psum x1 -> x0, waiting for transfers between devices: 115 us -> none  [on_device(): summed = lax.psum(partial_value, 'fs')]
    ppermute x0 -> x44, waiting for transfers between devices: none -> 89.2 us  [the longest x39 88.5 us: swap(): lax.ppermute(values, 'fs', [(rank, rank ^ offset) for rank in range(ranks)])]
    ppermute x0 -> x44, starting transfers between devices: none -> 47 us  [the longest x39 47 us: swap(): lax.ppermute(values, 'fs', [(rank, rank ^ offset) for rank in range(ranks)])]
    all_gather x1 -> x0, blocking collectives: 43.7 us -> none  [on_device(): all_directions = lax.all_gather(direction, 'fs', axis=0, tiled=True)]
    pallas_call x0 -> x4, Pallas kernels: none -> 21.6 us  [the longest x2 11.9 us: write_copies(): pl.pallas_call(functools.partial(copy_kernel, layout, bool(masters), len(...]
    unnamed x23 -> x52, local copies, waits for them, and re-layouts: 17.3 us -> 4.79 us
    dot_general x4 -> x0, matrix products: 7.34 us -> none  [the longest x1 3.74 us: on_device(): jnp.dot(normed, lax.all_gather(basis, 'fs', axis=0, tiled=True), preferre...]
  transfers between devices with their start and end apart: 4 -> 44, of which waited for: 4 -> 22; matrix products, arithmetic and copies ran while one was open for 3% -> 2% of each run, Pallas kernels for 0% -> 6%
where the time goes in v1:
time: 170 us
  waiting for transfers between devices  89.2 us (52%)
  starting transfers between devices  47 us (28%)
  Pallas kernels  21.6 us (13%)
  local copies, waits for them, and re-layouts  5.1 us (3%)
  other arithmetic  4.98 us (3%)
  between operations  1.86 us (1%)
    ppermute x39, waiting for transfers between devices, swap(): lax.ppermute(values, 'fs', [(rank, rank ^ offset) for rank in range(ranks)])  88.5 us
    ppermute x39, starting transfers between devices, swap(): lax.ppermute(values, 'fs', [(rank, rank ^ offset) for rank in range(ranks)])  47 us
    pallas_call x2, Pallas kernels, write_copies(): pl.pallas_call(functools.partial(copy_kernel, layout, bool(masters), len(...  11.9 us
    pallas_call x1, Pallas kernels, project(): pl.pallas_call(functools.partial(project_kernel, groups), in_specs=[pl.Bl...  7.77 us
    unnamed x52, local copies, waits for them, and re-layouts  4.79 us
  transfers between devices with their start and end apart: 44, of which 22 were waited for; matrix products, arithmetic and copies ran while one was open for 2% of the time, Pallas kernels for 6%

profile of v1, /device:TPU:0, one launch (start us, length us, event | category | flops | bytes accessed | tf_op | source)
XLA Modules:
  0.0 169.7 jit_solution(8415185594823398789)
XLA Ops:
  0.7 0.8 copy-done
  1.5 5.1 %collective-permute-start.2 = (bf16[128,128]{1,0:T(8,128)(2,1)S(1)}, bf16[128,128]{1,0:T(8,128)(2,1)S(1)}, u32[]{:S(2)}, u32[]{:S(2)}) collective-permute-start(bf16[128,128]{1,0:T(8,128)(2,1)S(1)} %constant_dynamic-slice_fusion), channel_id=1, source_target_pairs={{0,24},{2,26},{4,28},{6,30},{8,16},{10,18},{12,20},{14,22},{16,8},... | collective-permute-start | bytes 98312 | tf_op jit(solution)/shard_map/ppermute | solution.py:21
  7.1 1.3 collective-permute-done.2
  8.5 2.9 %collective-permute-done.1 = bf16[128,128]{1,0:T(8,128)(2,1)S(1)} collective-permute-done((bf16[128,128]{1,0:T(8,128)(2,1)S(1)}, bf16[128,128]{1,0:T(8,128)(2,1)S(1)}, u32[]{:S(2)}, u32[]{:S(2)}) %collective-permute-start.1) | collective-permute-done | bytes 32800 | tf_op jit(solution)/shard_map/ppermute | solution.py:21
  11.4 1.6 collective-permute-start.3
  13.0 1.5 collective-permute-start.4
  15.0 2.7 %collective-permute-done.3.refs_1_ = bf16[512,128]{1,0:T(8,128)(2,1)S(1)} collective-permute-done((bf16[512,128]{1,0:T(8,128)(2,1)S(1)}, bf16[512,128]{1,0:T(8,128)(2,1)S(1)}, u32[]{:S(2)}, u32[]{:S(2)}) %collective-permute-start.3) | collective-permute-done | bytes 131104 | tf_op jit(solution)/shard_map/ppermute | solution.py:21
  17.7 1.2 collective-permute-done.4.refs_2_
  18.9 1.4 collective-permute-done.5.refs_3_
  21.0 0.7 collective-permute-done.9.refs_7_
  21.8 0.6 copy-done.23
  22.4 7.8 %project.1 = (bf16[2048,256]{1,0:T(8,128)(2,1)}, f32[4,16,1536]{2,1,0:T(8,128)}, bf16[4,16,1536]{2,1,0:T(8,128)(2,1)}, bf16[4,16,1536]{2,1,0:T(8,128)(2,1)}, bf16[4,16,1536]{2,1,0:T(8,128)(2,1)}) custom-call(s32[2]{0:T(128)} %pad_add_fusion.where, bf16[512,128]{1,0:T(8,128)(2,1)} %copy-done.2, bf16[512,128]{1,0:T(8,128)(2,1)} %copy-done.17, ...), custom_call_target="tpu_custom_call" | custom-call | tf_op jit(solution)/shard_map/project/pallas_call | solution.py:180
  30.8 1.5 collective-permute-start.14
  32.3 1.5 collective-permute-start.13
  33.7 5.4 %collective-permute-done.15 = bf16[4,16,1536]{2,1,0:T(8,128)(2,1)S(1)} collective-permute-done((bf16[4,16,1536]{2,1,0:T(8,128)(2,1)}, bf16[4,16,1536]{2,1,0:T(8,128)(2,1)S(1)}, u32[]{:S(2)}, u32[]{:S(2)}) %collective-permute-start.15) | collective-permute-done | bytes 196640 | tf_op jit(solution)/shard_map/ppermute | solution.py:21
  39.2 3.0 %collective-permute-done.14 = bf16[4,16,1536]{2,1,0:T(8,128)(2,1)S(1)} collective-permute-done((bf16[4,16,1536]{2,1,0:T(8,128)(2,1)}, bf16[4,16,1536]{2,1,0:T(8,128)(2,1)S(1)}, u32[]{:S(2)}, u32[]{:S(2)}) %collective-permute-start.14) | collective-permute-done | bytes 196640 | tf_op jit(solution)/shard_map/ppermute | solution.py:21
  42.7 1.1 convert_add_fusion
  43.8 1.8 %collective-permute-start.18 = (bf16[16,1536]{1,0:T(8,128)(2,1)S(1)}, bf16[16,1536]{1,0:T(8,128)(2,1)S(1)}, u32[]{:S(2)}, u32[]{:S(2)}) collective-permute-start(bf16[16,1536]{1,0:T(8,128)(2,1)S(1)} %get-tuple-element.57), channel_id=1, source_target_pairs={{0,24},{2,26},{4,28},{6,30},{8,16},{10,18},{12,20},{14,22},{16,8},... | collective-permute-start | bytes 147464 | tf_op jit(solution)/shard_map/ppermute | solution.py:21
  46.0 2.3 %collective-permute-start.16 = (bf16[16,1536]{1,0:T(8,128)(2,1)S(1)}, bf16[16,1536]{1,0:T(8,128)(2,1)S(1)}, u32[]{:S(2)}, u32[]{:S(2)}) collective-permute-start(bf16[16,1536]{1,0:T(8,128)(2,1)S(1)} %get-tuple-element.56), channel_id=1, source_target_pairs={{0,8},{2,10},{4,12},{6,14},{8,0},{10,2},{12,4},{14,6},{16,24},{18,... | collective-permute-start | bytes 147464 | tf_op jit(solution)/shard_map/ppermute | solution.py:21
  48.3 1.9 %collective-permute-done.18 = bf16[16,1536]{1,0:T(8,128)(2,1)S(1)} collective-permute-done((bf16[16,1536]{1,0:T(8,128)(2,1)S(1)}, bf16[16,1536]{1,0:T(8,128)(2,1)S(1)}, u32[]{:S(2)}, u32[]{:S(2)}) %collective-permute-start.18) | collective-permute-done | bytes 49184 | tf_op jit(solution)/shard_map/ppermute | solution.py:21
  50.2 1.0 collective-permute-done.17
  51.2 2.3 %collective-permute-start.21 = (bf16[16,1536]{1,0:T(8,128)(2,1)S(1)}, bf16[16,1536]{1,0:T(8,128)(2,1)S(1)}, u32[]{:S(2)}, u32[]{:S(2)}) collective-permute-start(bf16[16,1536]{1,0:T(8,128)(2,1)S(1)} %get-tuple-element.50), channel_id=1, source_target_pairs={{0,24},{2,26},{4,28},{6,30},{8,16},{10,18},{12,20},{14,22},{16,8},... | collective-permute-start | bytes 147464 | tf_op jit(solution)/shard_map/ppermute | solution.py:21
  53.9 1.8 %collective-permute-start.19 = (bf16[16,1536]{1,0:T(8,128)(2,1)S(1)}, bf16[16,1536]{1,0:T(8,128)(2,1)S(1)}, u32[]{:S(2)}, u32[]{:S(2)}) collective-permute-start(bf16[16,1536]{1,0:T(8,128)(2,1)S(1)} %get-tuple-element.50), channel_id=1, source_target_pairs={{0,8},{2,10},{4,12},{6,14},{8,0},{10,2},{12,4},{14,6},{16,24},{18,... | collective-permute-start | bytes 147464 | tf_op jit(solution)/shard_map/ppermute | solution.py:21
  55.7 2.0 %collective-permute-done.21 = bf16[16,1536]{1,0:T(8,128)(2,1)S(1)} collective-permute-done((bf16[16,1536]{1,0:T(8,128)(2,1)S(1)}, bf16[16,1536]{1,0:T(8,128)(2,1)S(1)}, u32[]{:S(2)}, u32[]{:S(2)}) %collective-permute-start.21) | collective-permute-done | bytes 49184 | tf_op jit(solution)/shard_map/ppermute | solution.py:21
  57.7 1.1 collective-permute-done.20
  59.1 1.0 collective-permute-start.23
  60.1 1.6 collective-permute-start.24
  61.7 0.9 collective-permute-start.22
  62.6 2.0 %prepare.1 = (bf16[128,1536]{1,0:T(8,128)(2,1)}, bf16[16,3072]{1,0:T(8,128)(2,1)}) custom-call(f32[128,512]{1,0:T(8,128)} %refs_15_.1, f32[128,1024]{1,0:T(8,128)} %refs_16_.1, f32[16,512]{1,0:T(8,128)} %first_key.1, f32[16,512]{1,0:T(8,128)} %second_key.1, f32[16,1024]{1,0:T(8,128)} %first_value.1, f32[16,1024]{1,0:T(8,128)} %second_value.1), custom_call_target="tpu_custom_call" | custom-call | tf_op jit(solution)/shard_map/prepare/pallas_call | solution.py:78
  64.6 1.8 %collective-permute-start.12 = (bf16[16,3072]{1,0:T(8,128)(2,1)}, bf16[16,3072]{1,0:T(8,128)(2,1)S(1)}, u32[]{:S(2)}, u32[]{:S(2)}) collective-permute-start(bf16[16,3072]{1,0:T(8,128)(2,1)} %get-tuple-element.31), channel_id=1, source_target_pairs={{0,24},{2,26},{4,28},{6,30},{8,16},{10,18},{12,20},{14,22},{16,8},... | collective-permute-start | bytes 294920 | tf_op jit(solution)/shard_map/ppermute | solution.py:21
  66.4 0.7 collective-permute-start.11
  67.1 1.9 %collective-permute-start.10 = (bf16[16,3072]{1,0:T(8,128)(2,1)}, bf16[16,3072]{1,0:T(8,128)(2,1)S(1)}, u32[]{:S(2)}, u32[]{:S(2)}) collective-permute-start(bf16[16,3072]{1,0:T(8,128)(2,1)} %get-tuple-element.31), channel_id=1, source_target_pairs={{0,8},{2,10},{4,12},{6,14},{8,0},{10,2},{12,4},{14,6},{16,24},{18,... | collective-permute-start | bytes 294920 | tf_op jit(solution)/shard_map/ppermute | solution.py:21
  69.0 1.1 collective-permute-start.29
  70.2 2.1 %collective-permute-done.12 = bf16[16,3072]{1,0:T(8,128)(2,1)S(1)} collective-permute-done((bf16[16,3072]{1,0:T(8,128)(2,1)}, bf16[16,3072]{1,0:T(8,128)(2,1)S(1)}, u32[]{:S(2)}, u32[]{:S(2)}) %collective-permute-start.12) | collective-permute-done | bytes 98336 | tf_op jit(solution)/shard_map/ppermute | solution.py:21
  72.3 0.9 collective-permute-start.30
  73.2 1.5 collective-permute-done.11
  74.8 1.0 collective-permute-start.36
  75.8 0.9 maximum_convert_fusion
  76.7 11.6 %collective-permute-done.32.refs_7_ = bf16[128,1536]{1,0:T(8,128)(2,1)S(1)} collective-permute-done((bf16[128,1536]{1,0:T(8,128)(2,1)}, bf16[128,1536]{1,0:T(8,128)(2,1)S(1)}, u32[]{:S(2)}, u32[]{:S(2)}) %collective-permute-start.32) | collective-permute-done | bytes 393248 | tf_op jit(solution)/shard_map/ppermute | solution.py:21
  88.4 1.4 collective-permute-start.33
  91.3 0.7 collective-permute-start.26
  92.2 0.7 fusion.7
  92.9 0.6 fusion.11
  93.5 9.2 %collective-permute-done.26 = bf16[64,1536]{1,0:T(8,128)(2,1)S(1)} collective-permute-done((bf16[64,1536]{1,0:T(8,128)(2,1)S(1)}, bf16[64,1536]{1,0:T(8,128)(2,1)S(1)}, u32[]{:S(2)}, u32[]{:S(2)}) %collective-permute-start.26) | collective-permute-done | bytes 196640 | tf_op jit(solution)/shard_map/ppermute | solution.py:21
  102.7 1.3 collective-permute-start.27
  104.1 4.3 %collective-permute-done.27 = bf16[64,1536]{1,0:T(8,128)(2,1)S(1)} collective-permute-done((bf16[64,1536]{1,0:T(8,128)(2,1)S(1)}, bf16[64,1536]{1,0:T(8,128)(2,1)S(1)}, u32[]{:S(2)}, u32[]{:S(2)}) %collective-permute-start.27) | collective-permute-done | bytes 196640 | tf_op jit(solution)/shard_map/ppermute | solution.py:21
  108.3 1.1 collective-permute-start.28
  109.5 1.9 %collective-permute-start.34 = (bf16[128,1536]{1,0:T(8,128)(2,1)S(1)}, bf16[128,1536]{1,0:T(8,128)(2,1)}, u32[]{:S(2)}, u32[]{:S(2)}) collective-permute-start(bf16[128,1536]{1,0:T(8,128)(2,1)S(1)} %collective-permute-done.32.refs_7_), channel_id=1, source_target_pairs={{0,4},{2,6},{4,0},{6,2},{8,12},{10,14},{12,8},{14,10},{16,20},{18,... | collective-permute-start | bytes 1179656 | tf_op jit(solution)/shard_map/ppermute | solution.py:21
  111.3 0.6 collective-permute-start.31
  112.0 5.0 %collective-permute-done.28 = bf16[64,1536]{1,0:T(8,128)(2,1)S(1)} collective-permute-done((bf16[64,1536]{1,0:T(8,128)(2,1)S(1)}, bf16[64,1536]{1,0:T(8,128)(2,1)S(1)}, u32[]{:S(2)}, u32[]{:S(2)}) %collective-permute-start.28) | collective-permute-done | bytes 196640 | tf_op jit(solution)/shard_map/ppermute | solution.py:21
  117.0 1.4 collective-permute-start.37
  118.7 6.6 %collective-permute-done.31.refs_6_ = bf16[128,1536]{1,0:T(8,128)(2,1)S(1)} collective-permute-done((bf16[128,1536]{1,0:T(8,128)(2,1)S(1)}, bf16[128,1536]{1,0:T(8,128)(2,1)S(1)}, u32[]{:S(2)}, u32[]{:S(2)}) %collective-permute-start.31) | collective-permute-done | bytes 393248 | tf_op jit(solution)/shard_map/ppermute | solution.py:21
  125.3 0.8 copy-done.10
  126.1 7.2 %collective-permute-done.40.refs_3_ = bf16[128,1536]{1,0:T(8,128)(2,1)S(1)} collective-permute-done((bf16[128,1536]{1,0:T(8,128)(2,1)}, bf16[128,1536]{1,0:T(8,128)(2,1)S(1)}, u32[]{:S(2)}, u32[]{:S(2)}) %collective-permute-start.40) | collective-permute-done | bytes 393248 | tf_op jit(solution)/shard_map/ppermute | solution.py:21
  133.6 1.8 %collective-permute-start.42 = (bf16[128,1536]{1,0:T(8,128)(2,1)S(1)}, bf16[128,1536]{1,0:T(8,128)(2,1)S(1)}, u32[]{:S(2)}, u32[]{:S(2)}) collective-permute-start(bf16[128,1536]{1,0:T(8,128)(2,1)S(1)} %collective-permute-done.40.refs_3_), channel_id=1, source_target_pairs={{0,4},{2,6},{4,0},{6,2},{8,12},{10,14},{12,8},{14,10},{16,20},{18,... | collective-permute-start | bytes 1179656 | tf_op jit(solution)/shard_map/ppermute | solution.py:21
  135.4 1.4 collective-permute-start.43
  136.8 0.7 collective-permute-start.35
  137.5 1.4 collective-permute-start.39
  138.9 16.3 %collective-permute-done.35.refs_10_ = bf16[128,1536]{1,0:T(8,128)(2,1)S(1)} collective-permute-done((bf16[128,1536]{1,0:T(8,128)(2,1)}, bf16[128,1536]{1,0:T(8,128)(2,1)S(1)}, u32[]{:S(2)}, u32[]{:S(2)}) %collective-permute-start.35) | collective-permute-done | bytes 393248 | tf_op jit(solution)/shard_map/ppermute | solution.py:21
  155.2 0.7 copy-done.13
  156.0 0.7 copy-done.14
  156.7 8.1 %shard_map.177 = (bf16[2048,512]{1,0:T(8,128)(2,1)}, bf16[2048,1024]{1,0:T(8,128)(2,1)}, f32[128,512]{1,0:T(8,128)}, f32[128,1024]{1,0:T(8,128)}, f32[128,512]{1,0:T(8,128)}, /*index=5*/f32[128,1024]{1,0:T(8,128)}) custom-call(s32[1]{0:T(128)} %bitcast.refs_0_, bf16[2048,256]{1,0:T(8,128)(2,1)} %get-tuple-element.30.refs_1_, bf16[256,1536]{1,0:T(8,128)(2,1)} %copy-done.1, ...), custom_call_target="tpu_custom_call" | custom-call | tf_op jit(solution)/shard_map/pallas_call | solution.py:351
  164.9 0.7 copy-done.4
  165.9 3.8 %shard_map.178 = (bf16[2048,512]{1,0:T(8,128)(2,1)}, bf16[2048,1024]{1,0:T(8,128)(2,1)}) custom-call(s32[1]{0:T(128)} %bitcast.refs_0_, bf16[2048,256]{1,0:T(8,128)(2,1)} %get-tuple-element.30.refs_1_, bf16[256,1536]{1,0:T(8,128)(2,1)} %copy-done.1, bf16[128,1536]{1,0:T(8,128)(2,1)} %copy-done.3, ...), custom_call_target="tpu_custom_call", output_to_operand_aliasing={{0}: (7, {}), {1}: (8, {})} | custom-call | tf_op jit(solution)/shard_map/pallas_call | solution.py:351
  (120 shorter events, 6.0 us)
Async XLA Ops:
  0.6 0.8 copy-start
  1.5 7.0 %collective-permute-start.2 = (bf16[128,128]{1,0:T(8,128)(2,1)S(1)}, bf16[128,128]{1,0:T(8,128)(2,1)S(1)}, u32[]{:S(2)}, u32[]{:S(2)}) collective-permute-start(bf16[128,128]{1,0:T(8,128)(2,1)S(1)} %constant_dynamic-slice_fusion), channel_id=1, source_target_pairs={{0,24},{2,26},{4,28},{6,30},{8,16},{10,18},{12,20},{14,22},{16,8},... | collective-permute-start | bytes 98312 | tf_op jit(solution)/shard_map/ppermute | solution.py:21
  6.6 4.8 %collective-permute-start.1 = (bf16[128,128]{1,0:T(8,128)(2,1)S(1)}, bf16[128,128]{1,0:T(8,128)(2,1)S(1)}, u32[]{:S(2)}, u32[]{:S(2)}) collective-permute-start(bf16[128,128]{1,0:T(8,128)(2,1)S(1)} %constant_dynamic-slice_fusion), channel_id=1, source_target_pairs={{0,16},{2,18},{4,20},{6,22},{8,24},{10,26},{12,28},{14,30},{16,0},... | collective-permute-start | bytes 98312 | tf_op jit(solution)/shard_map/ppermute | solution.py:21
  6.6 4.8 %collective-permute-start = (bf16[128,128]{1,0:T(8,128)(2,1)S(1)}, bf16[128,128]{1,0:T(8,128)(2,1)S(1)}, u32[]{:S(2)}, u32[]{:S(2)}) collective-permute-start(bf16[128,128]{1,0:T(8,128)(2,1)S(1)} %constant_dynamic-slice_fusion), channel_id=1, source_target_pairs={{0,8},{2,10},{4,12},{6,14},{8,0},{10,2},{12,4},{14,6},{16,24},{18,... | collective-permute-start | bytes 98312 | tf_op jit(solution)/shard_map/ppermute | solution.py:21
  11.4 10.3 %copy-start.2 = (bf16[512,128]{1,0:T(8,128)(2,1)}, bf16[512,128]{1,0:T(8,128)(2,1)S(1)}, u32[]{:S(2)}) copy-start(bf16[512,128]{1,0:T(8,128)(2,1)S(1)} %pad_maximum_fusion.refs_0_) | copy-start | bytes 393220
  11.4 6.3 %collective-permute-start.3 = (bf16[512,128]{1,0:T(8,128)(2,1)S(1)}, bf16[512,128]{1,0:T(8,128)(2,1)S(1)}, u32[]{:S(2)}, u32[]{:S(2)}) collective-permute-start(bf16[512,128]{1,0:T(8,128)(2,1)S(1)} %pad_maximum_fusion.refs_0_), channel_id=1, source_target_pairs={{0,2},{2,0},{4,6},{6,4},{8,10},{10,8},{12,14},{14,12},{16,18},{18,... | collective-permute-start | bytes 393224 | tf_op jit(solution)/shard_map/ppermute | solution.py:21
  13.0 5.9 %collective-permute-start.4 = (bf16[512,128]{1,0:T(8,128)(2,1)S(1)}, bf16[512,128]{1,0:T(8,128)(2,1)S(1)}, u32[]{:S(2)}, u32[]{:S(2)}) collective-permute-start(bf16[512,128]{1,0:T(8,128)(2,1)S(1)} %pad_maximum_fusion.refs_0_), channel_id=1, source_target_pairs={{0,4},{2,6},{4,0},{6,2},{8,12},{10,14},{12,8},{14,10},{16,20},{18,... | collective-permute-start | bytes 393224 | tf_op jit(solution)/shard_map/ppermute | solution.py:21
  14.5 5.9 %collective-permute-start.5 = (bf16[512,128]{1,0:T(8,128)(2,1)S(1)}, bf16[512,128]{1,0:T(8,128)(2,1)S(1)}, u32[]{:S(2)}, u32[]{:S(2)}) collective-permute-start(bf16[512,128]{1,0:T(8,128)(2,1)S(1)} %pad_maximum_fusion.refs_0_), channel_id=1, source_target_pairs={{0,6},{2,4},{4,2},{6,0},{8,14},{10,12},{12,10},{14,8},{16,22},{18,... | collective-permute-start | bytes 393224 | tf_op jit(solution)/shard_map/ppermute | solution.py:21
  15.0 6.0 %collective-permute-start.6 = (bf16[512,128]{1,0:T(8,128)(2,1)S(1)}, bf16[512,128]{1,0:T(8,128)(2,1)S(1)}, u32[]{:S(2)}, u32[]{:S(2)}) collective-permute-start(bf16[512,128]{1,0:T(8,128)(2,1)S(1)} %pad_maximum_fusion.refs_0_), channel_id=1, source_target_pairs={{0,1},{1,0},{2,3},{3,2},{4,5},{5,4},{6,7},{7,6},{8,9},{9,8},{10,11... | collective-permute-start | bytes 393224 | tf_op jit(solution)/shard_map/ppermute | solution.py:97
  17.7 4.0 %copy-start.17 = (bf16[512,128]{1,0:T(8,128)(2,1)}, bf16[512,128]{1,0:T(8,128)(2,1)S(1)}, u32[]{:S(2)}) copy-start(bf16[512,128]{1,0:T(8,128)(2,1)S(1)} %collective-permute-done.3.refs_1_) | copy-start | bytes 393220
  17.7 3.3 %collective-permute-start.7 = (bf16[512,128]{1,0:T(8,128)(2,1)S(1)}, bf16[512,128]{1,0:T(8,128)(2,1)S(1)}, u32[]{:S(2)}, u32[]{:S(2)}) collective-permute-start(bf16[512,128]{1,0:T(8,128)(2,1)S(1)} %collective-permute-done.3.refs_1_), channel_id=1, source_target_pairs={{0,1},{1,0},{2,3},{3,2},{4,5},{5,4},{6,7},{7,6},{8,9},{9,8},{10,11... | collective-permute-start | bytes 393224 | tf_op jit(solution)/shard_map/ppermute | solution.py:97
  18.9 2.8 %copy-start.18 = (bf16[512,128]{1,0:T(8,128)(2,1)}, bf16[512,128]{1,0:T(8,128)(2,1)S(1)}, u32[]{:S(2)}) copy-start(bf16[512,128]{1,0:T(8,128)(2,1)S(1)} %collective-permute-done.4.refs_2_) | copy-start | bytes 393220
  18.9 2.1 %collective-permute-start.8 = (bf16[512,128]{1,0:T(8,128)(2,1)S(1)}, bf16[512,128]{1,0:T(8,128)(2,1)S(1)}, u32[]{:S(2)}, u32[]{:S(2)}) collective-permute-start(bf16[512,128]{1,0:T(8,128)(2,1)S(1)} %collective-permute-done.4.refs_2_), channel_id=1, source_target_pairs={{0,1},{1,0},{2,3},{3,2},{4,5},{5,4},{6,7},{7,6},{8,9},{9,8},{10,11... | collective-permute-start | bytes 393224 | tf_op jit(solution)/shard_map/ppermute | solution.py:97
  20.4 1.4 copy-start.19
  20.4 1.3 collective-permute-start.9
  21.0 0.8 copy-start.20
  21.0 0.8 copy-start.21
  30.2 9.0 %collective-permute-start.15 = (bf16[4,16,1536]{2,1,0:T(8,128)(2,1)}, bf16[4,16,1536]{2,1,0:T(8,128)(2,1)S(1)}, u32[]{:S(2)}, u32[]{:S(2)}) collective-permute-start(bf16[4,16,1536]{2,1,0:T(8,128)(2,1)} %get-tuple-element.35), channel_id=1, source_target_pairs={{0,6},{2,4},{4,2},{6,0},{8,14},{10,12},{12,10},{14,8},{16,22},{18,... | collective-permute-start | bytes 589832 | tf_op jit(solution)/shard_map/ppermute | solution.py:21
  30.8 11.4 %collective-permute-start.14 = (bf16[4,16,1536]{2,1,0:T(8,128)(2,1)}, bf16[4,16,1536]{2,1,0:T(8,128)(2,1)S(1)}, u32[]{:S(2)}, u32[]{:S(2)}) collective-permute-start(bf16[4,16,1536]{2,1,0:T(8,128)(2,1)} %get-tuple-element.34), channel_id=1, source_target_pairs={{0,4},{2,6},{4,0},{6,2},{8,12},{10,14},{12,8},{14,10},{16,20},{18,... | collective-permute-start | bytes 589832 | tf_op jit(solution)/shard_map/ppermute | solution.py:21
  32.3 10.4 %collective-permute-start.13 = (bf16[4,16,1536]{2,1,0:T(8,128)(2,1)}, bf16[4,16,1536]{2,1,0:T(8,128)(2,1)S(1)}, u32[]{:S(2)}, u32[]{:S(2)}) collective-permute-start(bf16[4,16,1536]{2,1,0:T(8,128)(2,1)} %get-tuple-element.33), channel_id=1, source_target_pairs={{0,2},{2,0},{4,6},{6,4},{8,10},{10,8},{12,14},{14,12},{16,18},{18,... | collective-permute-start | bytes 589832 | tf_op jit(solution)/shard_map/ppermute | solution.py:21
  43.8 48.4 %copy-start.15 = (f32[16,1024]{1,0:T(8,128)S(1)}, f32[16,1024]{1,0:T(8,128)}, u32[]{:S(2)}) copy-start(f32[16,1024]{1,0:T(8,128)} %first_value.1) | copy-start | bytes 196612
  43.8 48.4 %copy-start.16 = (f32[16,1024]{1,0:T(8,128)S(1)}, f32[16,1024]{1,0:T(8,128)}, u32[]{:S(2)}) copy-start(f32[16,1024]{1,0:T(8,128)} %second_value.1) | copy-start | bytes 196612
  43.8 49.0 %copy-start.24 = (f32[16,512]{1,0:T(8,128)S(1)}, f32[16,512]{1,0:T(8,128)}, u32[]{:S(2)}) copy-start(f32[16,512]{1,0:T(8,128)} %first_key.1) | copy-start | bytes 98308
  43.8 49.0 %copy-start.25 = (f32[16,512]{1,0:T(8,128)S(1)}, f32[16,512]{1,0:T(8,128)}, u32[]{:S(2)}) copy-start(f32[16,512]{1,0:T(8,128)} %second_key.1) | copy-start | bytes 98308
  43.8 6.4 %collective-permute-start.18 = (bf16[16,1536]{1,0:T(8,128)(2,1)S(1)}, bf16[16,1536]{1,0:T(8,128)(2,1)S(1)}, u32[]{:S(2)}, u32[]{:S(2)}) collective-permute-start(bf16[16,1536]{1,0:T(8,128)(2,1)S(1)} %get-tuple-element.57), channel_id=1, source_target_pairs={{0,24},{2,26},{4,28},{6,30},{8,16},{10,18},{12,20},{14,22},{16,8},... | collective-permute-start | bytes 147464 | tf_op jit(solution)/shard_map/ppermute | solution.py:21
  45.6 5.6 %collective-permute-start.17 = (bf16[16,1536]{1,0:T(8,128)(2,1)S(1)}, bf16[16,1536]{1,0:T(8,128)(2,1)S(1)}, u32[]{:S(2)}, u32[]{:S(2)}) collective-permute-start(bf16[16,1536]{1,0:T(8,128)(2,1)S(1)} %get-tuple-element.58), channel_id=1, source_target_pairs={{0,16},{2,18},{4,20},{6,22},{8,24},{10,26},{12,28},{14,30},{16,0},... | collective-permute-start | bytes 147464 | tf_op jit(solution)/shard_map/ppermute | solution.py:21
  46.0 5.2 %collective-permute-start.16 = (bf16[16,1536]{1,0:T(8,128)(2,1)S(1)}, bf16[16,1536]{1,0:T(8,128)(2,1)S(1)}, u32[]{:S(2)}, u32[]{:S(2)}) collective-permute-start(bf16[16,1536]{1,0:T(8,128)(2,1)S(1)} %get-tuple-element.56), channel_id=1, source_target_pairs={{0,8},{2,10},{4,12},{6,14},{8,0},{10,2},{12,4},{14,6},{16,24},{18,... | collective-permute-start | bytes 147464 | tf_op jit(solution)/shard_map/ppermute | solution.py:21
  51.2 6.5 %collective-permute-start.21 = (bf16[16,1536]{1,0:T(8,128)(2,1)S(1)}, bf16[16,1536]{1,0:T(8,128)(2,1)S(1)}, u32[]{:S(2)}, u32[]{:S(2)}) collective-permute-start(bf16[16,1536]{1,0:T(8,128)(2,1)S(1)} %get-tuple-element.50), channel_id=1, source_target_pairs={{0,24},{2,26},{4,28},{6,30},{8,16},{10,18},{12,20},{14,22},{16,8},... | collective-permute-start | bytes 147464 | tf_op jit(solution)/shard_map/ppermute | solution.py:21
  53.5 5.2 %collective-permute-start.20 = (bf16[16,1536]{1,0:T(8,128)(2,1)S(1)}, bf16[16,1536]{1,0:T(8,128)(2,1)S(1)}, u32[]{:S(2)}, u32[]{:S(2)}) collective-permute-start(bf16[16,1536]{1,0:T(8,128)(2,1)S(1)} %get-tuple-element.50), channel_id=1, source_target_pairs={{0,16},{2,18},{4,20},{6,22},{8,24},{10,26},{12,28},{14,30},{16,0},... | collective-permute-start | bytes 147464 | tf_op jit(solution)/shard_map/ppermute | solution.py:21
  53.9 4.8 %collective-permute-start.19 = (bf16[16,1536]{1,0:T(8,128)(2,1)S(1)}, bf16[16,1536]{1,0:T(8,128)(2,1)S(1)}, u32[]{:S(2)}, u32[]{:S(2)}) collective-permute-start(bf16[16,1536]{1,0:T(8,128)(2,1)S(1)} %get-tuple-element.50), channel_id=1, source_target_pairs={{0,8},{2,10},{4,12},{6,14},{8,0},{10,2},{12,4},{14,6},{16,24},{18,... | collective-permute-start | bytes 147464 | tf_op jit(solution)/shard_map/ppermute | solution.py:21
  59.1 8.0 %collective-permute-start.23 = (f32[16,128]{1,0:T(8,128)S(1)}, f32[16,128]{1,0:T(8,128)S(1)}, u32[]{:S(2)}, u32[]{:S(2)}) collective-permute-start(f32[16,128]{1,0:T(8,128)S(1)} %add_add_fusion.1), channel_id=1, source_target_pairs={{0,4},{2,6},{4,0},{6,2},{8,12},{10,14},{12,8},{14,10},{16,20},{18,... | collective-permute-start | bytes 24584 | tf_op jit(solution)/shard_map/ppermute | solution.py:21
  60.1 8.9 %collective-permute-start.24 = (f32[16,128]{1,0:T(8,128)S(1)}, f32[16,128]{1,0:T(8,128)S(1)}, u32[]{:S(2)}, u32[]{:S(2)}) collective-permute-start(f32[16,128]{1,0:T(8,128)S(1)} %add_add_fusion.1), channel_id=1, source_target_pairs={{0,6},{2,4},{4,2},{6,0},{8,14},{10,12},{12,10},{14,8},{16,22},{18,... | collective-permute-start | bytes 24584 | tf_op jit(solution)/shard_map/ppermute | solution.py:21
  61.7 8.4 %collective-permute-start.22 = (f32[16,128]{1,0:T(8,128)S(1)}, f32[16,128]{1,0:T(8,128)S(1)}, u32[]{:S(2)}, u32[]{:S(2)}) collective-permute-start(f32[16,128]{1,0:T(8,128)S(1)} %add_add_fusion.1), channel_id=1, source_target_pairs={{0,2},{2,0},{4,6},{6,4},{8,10},{10,8},{12,14},{14,12},{16,18},{18,... | collective-permute-start | bytes 24584 | tf_op jit(solution)/shard_map/ppermute | solution.py:21
  64.6 7.7 %collective-permute-start.12 = (bf16[16,3072]{1,0:T(8,128)(2,1)}, bf16[16,3072]{1,0:T(8,128)(2,1)S(1)}, u32[]{:S(2)}, u32[]{:S(2)}) collective-permute-start(bf16[16,3072]{1,0:T(8,128)(2,1)} %get-tuple-element.31), channel_id=1, source_target_pairs={{0,24},{2,26},{4,28},{6,30},{8,16},{10,18},{12,20},{14,22},{16,8},... | collective-permute-start | bytes 294920 | tf_op jit(solution)/shard_map/ppermute | solution.py:21
  66.4 8.4 %collective-permute-start.11 = (bf16[16,3072]{1,0:T(8,128)(2,1)}, bf16[16,3072]{1,0:T(8,128)(2,1)S(1)}, u32[]{:S(2)}, u32[]{:S(2)}) collective-permute-start(bf16[16,3072]{1,0:T(8,128)(2,1)} %get-tuple-element.31), channel_id=1, source_target_pairs={{0,16},{2,18},{4,20},{6,22},{8,24},{10,26},{12,28},{14,30},{16,0},... | collective-permute-start | bytes 294920 | tf_op jit(solution)/shard_map/ppermute | solution.py:21
  67.1 8.7 %collective-permute-start.10 = (bf16[16,3072]{1,0:T(8,128)(2,1)}, bf16[16,3072]{1,0:T(8,128)(2,1)S(1)}, u32[]{:S(2)}, u32[]{:S(2)}) collective-permute-start(bf16[16,3072]{1,0:T(8,128)(2,1)} %get-tuple-element.31), channel_id=1, source_target_pairs={{0,8},{2,10},{4,12},{6,14},{8,0},{10,2},{12,4},{14,6},{16,24},{18,... | collective-permute-start | bytes 294920 | tf_op jit(solution)/shard_map/ppermute | solution.py:21
  69.0 49.4 %collective-permute-start.29 = (bf16[128,1536]{1,0:T(8,128)(2,1)}, bf16[128,1536]{1,0:T(8,128)(2,1)S(1)}, u32[]{:S(2)}, u32[]{:S(2)}) collective-permute-start(bf16[128,1536]{1,0:T(8,128)(2,1)} %get-tuple-element.36.refs_3_), channel_id=1, source_target_pairs={{0,2},{2,0},{4,6},{6,4},{8,10},{10,8},{12,14},{14,12},{16,18},{18,... | collective-permute-start | bytes 1179656 | tf_op jit(solution)/shard_map/ppermute | solution.py:21
  70.1 18.3 %collective-permute-start.32 = (bf16[128,1536]{1,0:T(8,128)(2,1)}, bf16[128,1536]{1,0:T(8,128)(2,1)S(1)}, u32[]{:S(2)}, u32[]{:S(2)}) collective-permute-start(bf16[128,1536]{1,0:T(8,128)(2,1)} %get-tuple-element.36.refs_3_), channel_id=1, source_target_pairs={{0,8},{2,10},{4,12},{6,14},{8,0},{10,2},{12,4},{14,6},{16,24},{18,... | collective-permute-start | bytes 1179656 | tf_op jit(solution)/shard_map/ppermute | solution.py:21
  72.3 37.2 %collective-permute-start.30 = (bf16[128,1536]{1,0:T(8,128)(2,1)}, bf16[128,1536]{1,0:T(8,128)(2,1)S(1)}, u32[]{:S(2)}, u32[]{:S(2)}) collective-permute-start(bf16[128,1536]{1,0:T(8,128)(2,1)} %get-tuple-element.36.refs_3_), channel_id=1, source_target_pairs={{0,4},{2,6},{4,0},{6,2},{8,12},{10,14},{12,8},{14,10},{16,20},{18,... | collective-permute-start | bytes 1179656 | tf_op jit(solution)/shard_map/ppermute | solution.py:21
  74.8 36.6 %collective-permute-start.36 = (bf16[128,1536]{1,0:T(8,128)(2,1)}, bf16[128,1536]{1,0:T(8,128)(2,1)}, u32[]{:S(2)}, u32[]{:S(2)}) collective-permute-start(bf16[128,1536]{1,0:T(8,128)(2,1)} %get-tuple-element.36.refs_3_), channel_id=1, source_target_pairs={{0,16},{2,18},{4,20},{6,22},{8,24},{10,26},{12,28},{14,30},{16,0},... | collective-permute-start | bytes 1179656 | tf_op jit(solution)/shard_map/ppermute | solution.py:21
  75.8 14.0 %collective-permute-start.25 = (f32[16,128]{1,0:T(8,128)S(1)}, f32[16,128]{1,0:T(8,128)S(1)}, u32[]{:S(2)}, u32[]{:S(2)}) collective-permute-start(f32[16,128]{1,0:T(8,128)S(1)} %add_add_fusion), channel_id=1, source_target_pairs={{0,1},{1,0},{2,3},{3,2},{4,5},{5,4},{6,7},{7,6},{8,9},{9,8},{10,11... | collective-permute-start | bytes 24584 | tf_op jit(solution)/shard_map/ppermute | solution.py:235
  88.4 68.4 %copy-start.8 = (bf16[128,1536]{1,0:T(8,128)(2,1)}, bf16[128,1536]{1,0:T(8,128)(2,1)S(1)}, u32[]{:S(2)}) copy-start(bf16[128,1536]{1,0:T(8,128)(2,1)S(1)} %collective-permute-done.32.refs_7_) | copy-start | bytes 1179652
  88.4 45.2 %collective-permute-start.33 = (bf16[128,1536]{1,0:T(8,128)(2,1)S(1)}, bf16[128,1536]{1,0:T(8,128)(2,1)}, u32[]{:S(2)}, u32[]{:S(2)}) collective-permute-start(bf16[128,1536]{1,0:T(8,128)(2,1)S(1)} %collective-permute-done.32.refs_7_), channel_id=1, source_target_pairs={{0,2},{2,0},{4,6},{6,4},{8,10},{10,8},{12,14},{14,12},{16,18},{18,... | collective-permute-start | bytes 1179656 | tf_op jit(solution)/shard_map/ppermute | solution.py:21
  91.3 11.3 %collective-permute-start.26 = (bf16[64,1536]{1,0:T(8,128)(2,1)S(1)}, bf16[64,1536]{1,0:T(8,128)(2,1)S(1)}, u32[]{:S(2)}, u32[]{:S(2)}) collective-permute-start(bf16[64,1536]{1,0:T(8,128)(2,1)S(1)} %fusion.1), channel_id=1, source_target_pairs={{0,2},{2,0},{4,6},{6,4},{8,10},{10,8},{12,14},{14,12},{16,18},{18,... | collective-permute-start | bytes 589832 | tf_op jit(solution)/shard_map/ppermute | solution.py:21
  102.7 5.7 %collective-permute-start.27 = (bf16[64,1536]{1,0:T(8,128)(2,1)S(1)}, bf16[64,1536]{1,0:T(8,128)(2,1)S(1)}, u32[]{:S(2)}, u32[]{:S(2)}) collective-permute-start(bf16[64,1536]{1,0:T(8,128)(2,1)S(1)} %fusion.1), channel_id=1, source_target_pairs={{0,4},{2,6},{4,0},{6,2},{8,12},{10,14},{12,8},{14,10},{16,20},{18,... | collective-permute-start | bytes 589832 | tf_op jit(solution)/shard_map/ppermute | solution.py:21
  108.3 8.7 %collective-permute-start.28 = (bf16[64,1536]{1,0:T(8,128)(2,1)S(1)}, bf16[64,1536]{1,0:T(8,128)(2,1)S(1)}, u32[]{:S(2)}, u32[]{:S(2)}) collective-permute-start(bf16[64,1536]{1,0:T(8,128)(2,1)S(1)} %fusion.1), channel_id=1, source_target_pairs={{0,6},{2,4},{4,2},{6,0},{8,14},{10,12},{12,10},{14,8},{16,22},{18,... | collective-permute-start | bytes 589832 | tf_op jit(solution)/shard_map/ppermute | solution.py:21
  109.5 9.3 %copy-start.9 = (bf16[128,1536]{1,0:T(8,128)(2,1)}, bf16[128,1536]{1,0:T(8,128)(2,1)S(1)}, u32[]{:S(2)}) copy-start(bf16[128,1536]{1,0:T(8,128)(2,1)S(1)} %collective-permute-done.30.refs_5_) | copy-start | bytes 1179652
  109.5 25.9 %collective-permute-start.34 = (bf16[128,1536]{1,0:T(8,128)(2,1)S(1)}, bf16[128,1536]{1,0:T(8,128)(2,1)}, u32[]{:S(2)}, u32[]{:S(2)}) collective-permute-start(bf16[128,1536]{1,0:T(8,128)(2,1)S(1)} %collective-permute-done.32.refs_7_), channel_id=1, source_target_pairs={{0,4},{2,6},{4,0},{6,2},{8,12},{10,14},{12,8},{14,10},{16,20},{18,... | collective-permute-start | bytes 1179656 | tf_op jit(solution)/shard_map/ppermute | solution.py:21
  111.3 14.0 %collective-permute-start.31 = (bf16[128,1536]{1,0:T(8,128)(2,1)S(1)}, bf16[128,1536]{1,0:T(8,128)(2,1)S(1)}, u32[]{:S(2)}, u32[]{:S(2)}) collective-permute-start(bf16[128,1536]{1,0:T(8,128)(2,1)S(1)} %collective-permute-done.30.refs_5_), channel_id=1, source_target_pairs={{0,2},{2,0},{4,6},{6,4},{8,10},{10,8},{12,14},{14,12},{16,18},{18,... | collective-permute-start | bytes 1179656 | tf_op jit(solution)/shard_map/ppermute | solution.py:21
  117.0 19.8 %collective-permute-start.37 = (bf16[128,1536]{1,0:T(8,128)(2,1)}, bf16[128,1536]{1,0:T(8,128)(2,1)S(1)}, u32[]{:S(2)}, u32[]{:S(2)}) collective-permute-start(bf16[128,1536]{1,0:T(8,128)(2,1)} %collective-permute-done.36.refs_11_), channel_id=1, source_target_pairs={{0,2},{2,0},{4,6},{6,4},{8,10},{10,8},{12,14},{14,12},{16,18},{18,... | collective-permute-start | bytes 1179656 | tf_op jit(solution)/shard_map/ppermute | solution.py:21
  118.4 38.3 %copy-start.7 = (bf16[128,1536]{1,0:T(8,128)(2,1)}, bf16[128,1536]{1,0:T(8,128)(2,1)S(1)}, u32[]{:S(2)}) copy-start(bf16[128,1536]{1,0:T(8,128)(2,1)S(1)} %collective-permute-done.29.refs_4_) | copy-start | bytes 1179652
  118.5 19.0 %collective-permute-start.38 = (bf16[128,1536]{1,0:T(8,128)(2,1)}, bf16[128,1536]{1,0:T(8,128)(2,1)S(1)}, u32[]{:S(2)}, u32[]{:S(2)}) collective-permute-start(bf16[128,1536]{1,0:T(8,128)(2,1)} %collective-permute-done.36.refs_11_), channel_id=1, source_target_pairs={{0,4},{2,6},{4,0},{6,2},{8,12},{10,14},{12,8},{14,10},{16,20},{18,... | collective-permute-start | bytes 1179656 | tf_op jit(solution)/shard_map/ppermute | solution.py:21
  125.3 8.0 %collective-permute-start.40 = (bf16[128,1536]{1,0:T(8,128)(2,1)}, bf16[128,1536]{1,0:T(8,128)(2,1)S(1)}, u32[]{:S(2)}, u32[]{:S(2)}) collective-permute-start(bf16[128,1536]{1,0:T(8,128)(2,1)} %collective-permute-done.36.refs_11_), channel_id=1, source_target_pairs={{0,8},{2,10},{4,12},{6,14},{8,0},{10,2},{12,4},{14,6},{16,24},{18,... | collective-permute-start | bytes 1179656 | tf_op jit(solution)/shard_map/ppermute | solution.py:21
  133.3 31.6 %copy-start.3 = (bf16[128,1536]{1,0:T(8,128)(2,1)}, bf16[128,1536]{1,0:T(8,128)(2,1)S(1)}, u32[]{:S(2)}) copy-start(bf16[128,1536]{1,0:T(8,128)(2,1)S(1)} %collective-permute-done.40.refs_3_) | copy-start | bytes 1179652
  133.3 31.5 %collective-permute-start.41 = (bf16[128,1536]{1,0:T(8,128)(2,1)S(1)}, bf16[128,1536]{1,0:T(8,128)(2,1)S(1)}, u32[]{:S(2)}, u32[]{:S(2)}) collective-permute-start(bf16[128,1536]{1,0:T(8,128)(2,1)S(1)} %collective-permute-done.40.refs_3_), channel_id=1, source_target_pairs={{0,2},{2,0},{4,6},{6,4},{8,10},{10,8},{12,14},{14,12},{16,18},{18,... | collective-permute-start | bytes 1179656 | tf_op jit(solution)/shard_map/ppermute | solution.py:21
  133.6 31.3 %collective-permute-start.42 = (bf16[128,1536]{1,0:T(8,128)(2,1)S(1)}, bf16[128,1536]{1,0:T(8,128)(2,1)S(1)}, u32[]{:S(2)}, u32[]{:S(2)}) collective-permute-start(bf16[128,1536]{1,0:T(8,128)(2,1)S(1)} %collective-permute-done.40.refs_3_), channel_id=1, source_target_pairs={{0,4},{2,6},{4,0},{6,2},{8,12},{10,14},{12,8},{14,10},{16,20},{18,... | collective-permute-start | bytes 1179656 | tf_op jit(solution)/shard_map/ppermute | solution.py:21
  135.4 29.5 %collective-permute-start.43 = (bf16[128,1536]{1,0:T(8,128)(2,1)S(1)}, bf16[128,1536]{1,0:T(8,128)(2,1)S(1)}, u32[]{:S(2)}, u32[]{:S(2)}) collective-permute-start(bf16[128,1536]{1,0:T(8,128)(2,1)S(1)} %collective-permute-done.40.refs_3_), channel_id=1, source_target_pairs={{0,6},{2,4},{4,2},{6,0},{8,14},{10,12},{12,10},{14,8},{16,22},{18,... | collective-permute-start | bytes 1179656 | tf_op jit(solution)/shard_map/ppermute | solution.py:21
  136.8 2.1 %copy-start.11 = (bf16[128,1536]{1,0:T(8,128)(2,1)}, bf16[128,1536]{1,0:T(8,128)(2,1)S(1)}, u32[]{:S(2)}) copy-start(bf16[128,1536]{1,0:T(8,128)(2,1)S(1)} %collective-permute-done.37.refs_12_) | copy-start | bytes 1179652
  136.8 18.4 %collective-permute-start.35 = (bf16[128,1536]{1,0:T(8,128)(2,1)}, bf16[128,1536]{1,0:T(8,128)(2,1)S(1)}, u32[]{:S(2)}, u32[]{:S(2)}) collective-permute-start(bf16[128,1536]{1,0:T(8,128)(2,1)} %collective-permute-done.33.refs_8_), channel_id=1, source_target_pairs={{0,4},{2,6},{4,0},{6,2},{8,12},{10,14},{12,8},{14,10},{16,20},{18,... | collective-permute-start | bytes 1179656 | tf_op jit(solution)/shard_map/ppermute | solution.py:21
  137.5 17.7 %copy-start.12 = (bf16[128,1536]{1,0:T(8,128)(2,1)}, bf16[128,1536]{1,0:T(8,128)(2,1)S(1)}, u32[]{:S(2)}) copy-start(bf16[128,1536]{1,0:T(8,128)(2,1)S(1)} %collective-permute-done.38.refs_13_) | copy-start | bytes 1179652
  137.5 17.7 %collective-permute-start.39 = (bf16[128,1536]{1,0:T(8,128)(2,1)S(1)}, bf16[128,1536]{1,0:T(8,128)(2,1)S(1)}, u32[]{:S(2)}, u32[]{:S(2)}) collective-permute-start(bf16[128,1536]{1,0:T(8,128)(2,1)S(1)} %collective-permute-done.38.refs_13_), channel_id=1, source_target_pairs={{0,2},{2,0},{4,6},{6,4},{8,10},{10,8},{12,14},{14,12},{16,18},{18,... | collective-permute-start | bytes 1179656 | tf_op jit(solution)/shard_map/ppermute | solution.py:21
  138.9 17.8 %copy-start.1 = (bf16[256,1536]{1,0:T(8,128)(2,1)}, bf16[256,1536]{1,0:T(8,128)(2,1)S(1)}, u32[]{:S(2)}) copy-start(bf16[256,1536]{1,0:T(8,128)(2,1)S(1)} %slice_dynamic-update-slice_fusion.refs_2_) | copy-start | bytes 2359300
  164.9 0.9 copy-start.5
  164.9 1.0 copy-start.6
  (6 other events, 4.4 us)

commit v2 on v1

--- a/solution.py
+++ b/solution.py
@@ -62,6 +62,10 @@
     return chunks
 
 
+def in_vmem(*arrays):
+    return [pltpu.with_memory_space_constraint(array, pltpu.VMEM) for array in arrays]
+
+
 def prepare_kernel(master_key, master_value, first_key, second_key, first_value, second_value, master, moments):
     key_cols = master_key.shape[1]
     cols = master.shape[1]
@@ -98,10 +102,10 @@
     return mine, theirs
 
 
-PARTS = 2
-
-
-def project_kernel(groups, where, *refs):
+PARTS = 4
+
+
+def project_kernel(groups, *refs):
     mine, theirs, refs = refs[:INNER], refs[INNER : 2 * INNER], refs[2 * INNER :]
     normed, key_cot, value_cot, whole_out, home, *aways = refs[: 5 + INNER - 1]
     tokens, cots, upper, whole, partial, home_buf, away_buf, token_sem, cot_sem, give_sem = refs[5 + INNER - 1 :]
@@ -121,7 +125,7 @@
     ]
     for load in cot_loads:
         load.start()
-    me, core = where[0], where[1]
+    me, core = lax.axis_index("fs"), lax.axis_index("tp") % 2
     half = mine[0].shape[1]
     rows = mine[0].shape[0] // groups
     for first in range(2):
@@ -171,7 +175,6 @@
     groups = ranks // INNER
     low_rows = depth // ranks
     cols = key_cot.shape[1] + value_cot.shape[1]
-    where = jnp.stack([me, lax.axis_index("tp") % 2]).astype(jnp.int32)
     local = pl.BlockSpec(memory_space=pltpu.VMEM)
     anywhere = pl.BlockSpec(memory_space=pl.ANY)
     tidy = low_rows % 8 == 0
@@ -179,7 +182,7 @@
     away = jax.ShapeDtypeStruct((groups, low_rows, cols) if tidy else (8, 128), jnp.bfloat16)
     whole, home, *aways = pl.pallas_call(
         functools.partial(project_kernel, groups),
-        in_specs=[pl.BlockSpec(memory_space=pltpu.SMEM)] + [local] * (2 * INNER) + [anywhere] * 3,
+        in_specs=[local] * (2 * INNER) + [anywhere] * 3,
         out_specs=[anywhere] * 2 + [anywhere if tidy else local] * (INNER - 1),
         out_shape=[jax.ShapeDtypeStruct((normed.shape[1], depth), jnp.bfloat16), home] + [away] * (INNER - 1),
         scratch_shapes=[
@@ -195,7 +198,7 @@
             pltpu.SemaphoreType.DMA((INNER + 1,)),
         ],
         name="project",
-    )(where, *mine, *theirs, normed, key_cot, value_cot)
+    )(*in_vmem(*mine, *theirs), normed, key_cot, value_cot)
     if not tidy:
         blocks = home.reshape(groups, INNER, low_rows, cols)
         inner = me % INNER
@@ -238,7 +241,7 @@
 
 def copy_kernel(layout, with_own, inherited, *refs):
     count = sum(len(parts) for _, parts in layout)
-    order, basis, directions, *rest = refs
+    basis, directions, *rest = refs
     pieces, rest = rest[:count], rest[count:]
     masters, rest = (rest[:2], rest[2:]) if with_own else ((), rest)
     rest = rest[inherited:]
@@ -247,13 +250,15 @@
     taken, made, step, take_sem, key_sem, value_sem, *rest = rest
     rows = step.shape[0] // INNER
     key_cols = copy_key.shape[1]
-    here = order[0]
+    here = lax.axis_index("fs")
     inner = here % INNER
     outer = here // INNER
-    takes = [
-        pltpu.make_async_copy(piece, taken.at[slot, pl.ds(0, piece.shape[0])], take_sem.at[slot])
-        for slot, piece in enumerate(pieces)
-    ]
+    takes = []
+    if with_own:
+        takes = [
+            pltpu.make_async_copy(piece, taken.at[slot, pl.ds(0, piece.shape[0])], take_sem.at[slot])
+            for slot, piece in enumerate(pieces)
+        ]
     for take in takes:
         take.start()
     if with_own:
@@ -281,9 +286,13 @@
                     directions[...],
                     preferred_element_type=jnp.float32,
                 )
-            takes[slot].wait()
+            if takes:
+                takes[slot].wait()
+                piece = taken[slot, pl.ds(0, size)]
+            else:
+                piece = pieces[slot][...]
             change = learn_rate * step[pl.ds(spot, size), :]
-            made[slot, pl.ds(0, size)] = (taken[slot, pl.ds(0, size)].astype(jnp.float32) - change).astype(jnp.bfloat16)
+            made[slot, pl.ds(0, size)] = (piece.astype(jnp.float32) - change).astype(jnp.bfloat16)
             target = pl.ds(pl.multiple_of(first_row + spot, size), size)
             for out_ref, columns, sem in (
                 (copy_key, pl.ds(0, key_cols), key_sem),
@@ -317,7 +326,7 @@
         give.wait()
 
 
-def write_copies(chunks, masters, me, basis, directions, key_cols, ranks, earlier):
+def write_copies(chunks, masters, basis, directions, key_cols, ranks, earlier):
     rows = basis.shape[0] // ranks
     cols = directions.shape[1]
     layout = tuple((chunk, tuple((away, start) for away, start, _ in parts)) for chunk, parts in chunks)
@@ -347,16 +356,17 @@
             pltpu.SemaphoreType.DMA((2,)),
             pltpu.SemaphoreType.DMA((4,)),
         ]
-    first_alias = 3 + count + len(masters)
+    first_alias = 2 + count + len(masters)
     return pl.pallas_call(
         functools.partial(copy_kernel, layout, bool(masters), len(earlier)),
-        in_specs=[pl.BlockSpec(memory_space=pltpu.SMEM), local, local]
-        + [anywhere] * (count + len(masters) + len(earlier)),
+        in_specs=[local, local]
+        + [anywhere if masters else local] * count
+        + [anywhere] * (len(masters) + len(earlier)),
         out_specs=[anywhere] * len(out_shape),
         out_shape=out_shape,
         scratch_shapes=scratch,
         input_output_aliases={first_alias: 0, first_alias + 1: 1} if earlier else {},
-    )(me.reshape(1), basis, directions, *pieces, *masters, *earlier)
+    )(basis, *in_vmem(directions), *(pieces if masters else in_vmem(*pieces)), *masters, *earlier)
 
 
 def on_device(
@@ -404,10 +414,10 @@
     new_first_key, new_second_key = advance(low[:, :key_cols], first_key, second_key)
     new_first_value, new_second_value = advance(low[:, key_cols:], first_value, second_value)
     copy_key, copy_value, *own = write_copies(
-        chunks[:-1], (master_key, master_value), me, whole_basis, directions, key_cols, ranks, ()
+        chunks[:-1], (master_key, master_value), whole_basis, directions, key_cols, ranks, ()
     )
     copy_key, copy_value = write_copies(
-        chunks[-1:], (), me, whole_basis, directions, key_cols, ranks, (copy_key, copy_value)
+        chunks[-1:], (), whole_basis, directions, key_cols, ranks, (copy_key, copy_value)
     )
     return (*own, copy_key, copy_value, new_first_key, new_second_key, new_first_value, new_second_value)
 

time: 170 us -> 166 us (0.976)
  waiting for transfers between devices: 89.2 us -> 91.7 us
  local copies, waits for them, and re-layouts: 5.1 us -> 2.68 us
  Pallas kernels: 21.6 us -> 19.6 us
    unnamed x52 -> x28, local copies, waits for them, and re-layouts: 4.79 us -> 2.37 us
    ppermute x39, waiting for transfers between devices: 88.5 us -> 90.3 us  [swap(): lax.ppermute(values, 'fs', [(rank, rank ^ offset) for rank in range(ranks)])]
where the time goes in v2:
time: 166 us
  waiting for transfers between devices  91.7 us (55%)
  starting transfers between devices  45.7 us (28%)
  Pallas kernels  19.6 us (12%)
  other arithmetic  4.39 us (3%)
  local copies, waits for them, and re-layouts  2.68 us (2%)
  between operations  1.76 us (1%)
    ppermute x39, waiting for transfers between devices, swap(): lax.ppermute(values, 'fs', [(rank, rank ^ offset) for rank in range(ranks)])  90.3 us
    ppermute x39, starting transfers between devices, swap(): lax.ppermute(values, 'fs', [(rank, rank ^ offset) for rank in range(ranks)])  45.7 us
    pallas_call x2, Pallas kernels, write_copies(): pl.pallas_call(functools.partial(copy_kernel, layout, bool(masters), len(...  11.4 us
    pallas_call x1, Pallas kernels, project(): pl.pallas_call(functools.partial(project_kernel, groups), in_specs=[local...  6.31 us
  transfers between devices with their start and end apart: 44, of which 22 were waited for; matrix products, arithmetic and copies ran while one was open for 2% of the time, Pallas kernels for 6%

profile of v2, /device:TPU:0, one launch (start us, length us, event | category | flops | bytes accessed | tf_op | source)
XLA Modules:
  0.0 165.8 jit_solution(10005919298592622046)
XLA Ops:
  0.7 0.8 copy-done
  1.5 5.1 %collective-permute-start.2 = (bf16[128,128]{1,0:T(8,128)(2,1)S(1)}, bf16[128,128]{1,0:T(8,128)(2,1)S(1)}, u32[]{:S(2)}, u32[]{:S(2)}) collective-permute-start(bf16[128,128]{1,0:T(8,128)(2,1)S(1)} %constant_dynamic-slice_fusion), channel_id=1, source_target_pairs={{0,24},{2,26},{4,28},{6,30},{8,16},{10,18},{12,20},{14,22},{16,8},... | collective-permute-start | bytes 98312 | tf_op jit(solution)/shard_map/ppermute | solution.py:21
  6.6 0.6 collective-permute-start
  7.1 1.3 collective-permute-done.2
  8.5 2.9 %collective-permute-done.1 = bf16[128,128]{1,0:T(8,128)(2,1)S(1)} collective-permute-done((bf16[128,128]{1,0:T(8,128)(2,1)S(1)}, bf16[128,128]{1,0:T(8,128)(2,1)S(1)}, u32[]{:S(2)}, u32[]{:S(2)}) %collective-permute-start.1) | collective-permute-done | bytes 32800 | tf_op jit(solution)/shard_map/ppermute | solution.py:21
  11.4 1.6 collective-permute-start.3
  13.0 1.5 collective-permute-start.4
  15.0 2.7 %collective-permute-done.3.refs_1_ = bf16[512,128]{1,0:T(8,128)(2,1)S(1)} collective-permute-done((bf16[512,128]{1,0:T(8,128)(2,1)S(1)}, bf16[512,128]{1,0:T(8,128)(2,1)S(1)}, u32[]{:S(2)}, u32[]{:S(2)}) %collective-permute-start.3) | collective-permute-done | bytes 131104 | tf_op jit(solution)/shard_map/ppermute | solution.py:21
  17.7 1.2 collective-permute-done.4.refs_2_
  18.9 1.4 collective-permute-done.5.refs_3_
  20.4 1.3 collective-permute-done.9.refs_7_
  21.7 6.3 %project.1 = (bf16[2048,256]{1,0:T(8,128)(2,1)}, f32[4,16,1536]{2,1,0:T(8,128)}, bf16[4,16,1536]{2,1,0:T(8,128)(2,1)}, bf16[4,16,1536]{2,1,0:T(8,128)(2,1)}, bf16[4,16,1536]{2,1,0:T(8,128)(2,1)}) custom-call(bf16[512,128]{1,0:T(8,128)(2,1)S(1)} %pad_maximum_fusion.refs_0_, bf16[512,128]{1,0:T(8,128)(2,1)S(1)} %collective-permute-done.3.refs_1_, ...), custom_call_target="tpu_custom_call" | custom-call | tf_op jit(solution)/shard_map/project/pallas_call | solution.py:183
  28.0 0.6 collective-permute-start.15
  28.6 1.5 collective-permute-start.14
  30.1 1.5 collective-permute-start.13
  31.6 5.4 %collective-permute-done.15 = bf16[4,16,1536]{2,1,0:T(8,128)(2,1)S(1)} collective-permute-done((bf16[4,16,1536]{2,1,0:T(8,128)(2,1)}, bf16[4,16,1536]{2,1,0:T(8,128)(2,1)S(1)}, u32[]{:S(2)}, u32[]{:S(2)}) %collective-permute-start.15) | collective-permute-done | bytes 196640 | tf_op jit(solution)/shard_map/ppermute | solution.py:21
  37.0 2.7 %collective-permute-done.14 = bf16[4,16,1536]{2,1,0:T(8,128)(2,1)S(1)} collective-permute-done((bf16[4,16,1536]{2,1,0:T(8,128)(2,1)}, bf16[4,16,1536]{2,1,0:T(8,128)(2,1)S(1)}, u32[]{:S(2)}, u32[]{:S(2)}) %collective-permute-start.14) | collective-permute-done | bytes 196640 | tf_op jit(solution)/shard_map/ppermute | solution.py:21
  39.7 0.6 collective-permute-done.13
  40.3 1.1 convert_add_fusion
  41.5 1.8 %collective-permute-start.18 = (bf16[16,1536]{1,0:T(8,128)(2,1)S(1)}, bf16[16,1536]{1,0:T(8,128)(2,1)S(1)}, u32[]{:S(2)}, u32[]{:S(2)}) collective-permute-start(bf16[16,1536]{1,0:T(8,128)(2,1)S(1)} %get-tuple-element.57), channel_id=1, source_target_pairs={{0,24},{2,26},{4,28},{6,30},{8,16},{10,18},{12,20},{14,22},{16,8},... | collective-permute-start | bytes 147464 | tf_op jit(solution)/shard_map/ppermute | solution.py:21
  43.6 2.3 %collective-permute-start.16 = (bf16[16,1536]{1,0:T(8,128)(2,1)S(1)}, bf16[16,1536]{1,0:T(8,128)(2,1)S(1)}, u32[]{:S(2)}, u32[]{:S(2)}) collective-permute-start(bf16[16,1536]{1,0:T(8,128)(2,1)S(1)} %get-tuple-element.56), channel_id=1, source_target_pairs={{0,8},{2,10},{4,12},{6,14},{8,0},{10,2},{12,4},{14,6},{16,24},{18,... | collective-permute-start | bytes 147464 | tf_op jit(solution)/shard_map/ppermute | solution.py:21
  45.9 1.8 %collective-permute-done.18 = bf16[16,1536]{1,0:T(8,128)(2,1)S(1)} collective-permute-done((bf16[16,1536]{1,0:T(8,128)(2,1)S(1)}, bf16[16,1536]{1,0:T(8,128)(2,1)S(1)}, u32[]{:S(2)}, u32[]{:S(2)}) %collective-permute-start.18) | collective-permute-done | bytes 49184 | tf_op jit(solution)/shard_map/ppermute | solution.py:21
  47.7 1.1 collective-permute-done.17
  48.8 2.5 %collective-permute-start.21 = (bf16[16,1536]{1,0:T(8,128)(2,1)S(1)}, bf16[16,1536]{1,0:T(8,128)(2,1)S(1)}, u32[]{:S(2)}, u32[]{:S(2)}) collective-permute-start(bf16[16,1536]{1,0:T(8,128)(2,1)S(1)} %get-tuple-element.50), channel_id=1, source_target_pairs={{0,24},{2,26},{4,28},{6,30},{8,16},{10,18},{12,20},{14,22},{16,8},... | collective-permute-start | bytes 147464 | tf_op jit(solution)/shard_map/ppermute | solution.py:21
  51.6 1.7 %collective-permute-start.19 = (bf16[16,1536]{1,0:T(8,128)(2,1)S(1)}, bf16[16,1536]{1,0:T(8,128)(2,1)S(1)}, u32[]{:S(2)}, u32[]{:S(2)}) collective-permute-start(bf16[16,1536]{1,0:T(8,128)(2,1)S(1)} %get-tuple-element.50), channel_id=1, source_target_pairs={{0,8},{2,10},{4,12},{6,14},{8,0},{10,2},{12,4},{14,6},{16,24},{18,... | collective-permute-start | bytes 147464 | tf_op jit(solution)/shard_map/ppermute | solution.py:21
  53.3 1.7 %collective-permute-done.21 = bf16[16,1536]{1,0:T(8,128)(2,1)S(1)} collective-permute-done((bf16[16,1536]{1,0:T(8,128)(2,1)S(1)}, bf16[16,1536]{1,0:T(8,128)(2,1)S(1)}, u32[]{:S(2)}, u32[]{:S(2)}) %collective-permute-start.21) | collective-permute-done | bytes 49184 | tf_op jit(solution)/shard_map/ppermute | solution.py:21
  54.9 1.4 collective-permute-done.20
  56.7 1.1 collective-permute-start.23
  57.7 1.5 collective-permute-start.24
  59.3 1.0 collective-permute-start.22
  60.2 1.9 %prepare.1 = (bf16[128,1536]{1,0:T(8,128)(2,1)}, bf16[16,3072]{1,0:T(8,128)(2,1)}) custom-call(f32[128,512]{1,0:T(8,128)} %refs_14_.1, f32[128,1024]{1,0:T(8,128)} %refs_15_.1, f32[16,512]{1,0:T(8,128)} %first_key.1, f32[16,512]{1,0:T(8,128)} %second_key.1, f32[16,1024]{1,0:T(8,128)} %first_value.1, f32[16,1024]{1,0:T(8,128)} %second_value.1), custom_call_target="tpu_custom_call" | custom-call | tf_op jit(solution)/shard_map/prepare/pallas_call | solution.py:82
  62.2 1.9 %collective-permute-start.12 = (bf16[16,3072]{1,0:T(8,128)(2,1)}, bf16[16,3072]{1,0:T(8,128)(2,1)S(1)}, u32[]{:S(2)}, u32[]{:S(2)}) collective-permute-start(bf16[16,3072]{1,0:T(8,128)(2,1)} %get-tuple-element.31), channel_id=1, source_target_pairs={{0,24},{2,26},{4,28},{6,30},{8,16},{10,18},{12,20},{14,22},{16,8},... | collective-permute-start | bytes 294920 | tf_op jit(solution)/shard_map/ppermute | solution.py:21
  64.1 0.5 collective-permute-start.11
  64.7 1.9 %collective-permute-start.10 = (bf16[16,3072]{1,0:T(8,128)(2,1)}, bf16[16,3072]{1,0:T(8,128)(2,1)S(1)}, u32[]{:S(2)}, u32[]{:S(2)}) collective-permute-start(bf16[16,3072]{1,0:T(8,128)(2,1)} %get-tuple-element.31), channel_id=1, source_target_pairs={{0,8},{2,10},{4,12},{6,14},{8,0},{10,2},{12,4},{14,6},{16,24},{18,... | collective-permute-start | bytes 294920 | tf_op jit(solution)/shard_map/ppermute | solution.py:21
  66.6 1.0 collective-permute-start.29
  67.7 2.2 %collective-permute-done.12 = bf16[16,3072]{1,0:T(8,128)(2,1)S(1)} collective-permute-done((bf16[16,3072]{1,0:T(8,128)(2,1)}, bf16[16,3072]{1,0:T(8,128)(2,1)S(1)}, u32[]{:S(2)}, u32[]{:S(2)}) %collective-permute-start.12) | collective-permute-done | bytes 98336 | tf_op jit(solution)/shard_map/ppermute | solution.py:21
  69.9 1.0 collective-permute-start.30
  70.9 1.4 collective-permute-done.11
  72.3 0.9 collective-permute-start.36
  73.2 0.9 maximum_convert_fusion
  74.2 11.8 %collective-permute-done.32.refs_6_ = bf16[128,1536]{1,0:T(8,128)(2,1)S(1)} collective-permute-done((bf16[128,1536]{1,0:T(8,128)(2,1)}, bf16[128,1536]{1,0:T(8,128)(2,1)S(1)}, u32[]{:S(2)}, u32[]{:S(2)}) %collective-permute-start.32) | collective-permute-done | bytes 393248 | tf_op jit(solution)/shard_map/ppermute | solution.py:21
  86.0 0.6 collective-permute-start.33
  86.5 0.6 add_reduce_fusion
  88.1 1.5 collective-permute-start.26
  89.8 0.7 fusion.7
  90.5 0.6 fusion.11
  91.1 9.2 %collective-permute-done.26 = bf16[64,1536]{1,0:T(8,128)(2,1)S(1)} collective-permute-done((bf16[64,1536]{1,0:T(8,128)(2,1)S(1)}, bf16[64,1536]{1,0:T(8,128)(2,1)S(1)}, u32[]{:S(2)}, u32[]{:S(2)}) %collective-permute-start.26) | collective-permute-done | bytes 196640 | tf_op jit(solution)/shard_map/ppermute | solution.py:21
  100.3 1.1 collective-permute-start.27
  101.5 4.5 %collective-permute-done.27 = bf16[64,1536]{1,0:T(8,128)(2,1)S(1)} collective-permute-done((bf16[64,1536]{1,0:T(8,128)(2,1)S(1)}, bf16[64,1536]{1,0:T(8,128)(2,1)S(1)}, u32[]{:S(2)}, u32[]{:S(2)}) %collective-permute-start.27) | collective-permute-done | bytes 196640 | tf_op jit(solution)/shard_map/ppermute | solution.py:21
  106.0 0.8 collective-permute-start.28
  106.9 1.2 collective-permute-start.34
  108.1 1.6 collective-permute-start.31
  109.6 5.0 %collective-permute-done.28 = bf16[64,1536]{1,0:T(8,128)(2,1)S(1)} collective-permute-done((bf16[64,1536]{1,0:T(8,128)(2,1)S(1)}, bf16[64,1536]{1,0:T(8,128)(2,1)S(1)}, u32[]{:S(2)}, u32[]{:S(2)}) %collective-permute-start.28) | collective-permute-done | bytes 196640 | tf_op jit(solution)/shard_map/ppermute | solution.py:21
  115.2 1.0 collective-permute-start.38
  116.1 6.6 %collective-permute-done.31.refs_5_ = bf16[128,1536]{1,0:T(8,128)(2,1)S(1)} collective-permute-done((bf16[128,1536]{1,0:T(8,128)(2,1)S(1)}, bf16[128,1536]{1,0:T(8,128)(2,1)S(1)}, u32[]{:S(2)}, u32[]{:S(2)}) %collective-permute-start.31) | collective-permute-done | bytes 393248 | tf_op jit(solution)/shard_map/ppermute | solution.py:21
  122.7 8.0 %collective-permute-done.40.refs_2_ = bf16[128,1536]{1,0:T(8,128)(2,1)S(1)} collective-permute-done((bf16[128,1536]{1,0:T(8,128)(2,1)}, bf16[128,1536]{1,0:T(8,128)(2,1)S(1)}, u32[]{:S(2)}, u32[]{:S(2)}) %collective-permute-start.40) | collective-permute-done | bytes 393248 | tf_op jit(solution)/shard_map/ppermute | solution.py:21
  131.0 1.1 collective-permute-start.42
  132.1 2.1 %collective-permute-start.43 = (bf16[128,1536]{1,0:T(8,128)(2,1)S(1)}, bf16[128,1536]{1,0:T(8,128)(2,1)S(1)}, u32[]{:S(2)}, u32[]{:S(2)}) collective-permute-start(bf16[128,1536]{1,0:T(8,128)(2,1)S(1)} %collective-permute-done.40.refs_2_), channel_id=1, source_target_pairs={{0,6},{2,4},{4,2},{6,0},{8,14},{10,12},{12,10},{14,8},{16,22},{18,... | collective-permute-start | bytes 1179656 | tf_op jit(solution)/shard_map/ppermute | solution.py:21
  134.2 0.9 collective-permute-start.35
  135.6 17.2 %collective-permute-done.35.refs_9_ = bf16[128,1536]{1,0:T(8,128)(2,1)S(1)} collective-permute-done((bf16[128,1536]{1,0:T(8,128)(2,1)}, bf16[128,1536]{1,0:T(8,128)(2,1)S(1)}, u32[]{:S(2)}, u32[]{:S(2)}) %collective-permute-start.35) | collective-permute-done | bytes 393248 | tf_op jit(solution)/shard_map/ppermute | solution.py:21
  152.9 0.7 copy-done.8
  153.6 0.8 copy-done.9
  154.4 8.0 %shard_map.177 = (bf16[2048,512]{1,0:T(8,128)(2,1)}, bf16[2048,1024]{1,0:T(8,128)(2,1)}, f32[128,512]{1,0:T(8,128)}, f32[128,1024]{1,0:T(8,128)}, f32[128,512]{1,0:T(8,128)}, /*index=5*/f32[128,1024]{1,0:T(8,128)}) custom-call(bf16[2048,256]{1,0:T(8,128)(2,1)} %get-tuple-element.30.refs_0_, bf16[256,1536]{1,0:T(8,128)(2,1)S(1)} %slice_dynamic-update-slice_fusion.refs_1_, ...), custom_call_target="tpu_custom_call" | custom-call | tf_op jit(solution)/shard_map/pallas_call | solution.py:360
  162.5 3.4 %shard_map.178 = (bf16[2048,512]{1,0:T(8,128)(2,1)}, bf16[2048,1024]{1,0:T(8,128)(2,1)}) custom-call(bf16[2048,256]{1,0:T(8,128)(2,1)} %get-tuple-element.30.refs_0_, bf16[256,1536]{1,0:T(8,128)(2,1)S(1)} %slice_dynamic-update-slice_fusion.refs_1_, ...), custom_call_target="tpu_custom_call", output_to_operand_aliasing={{0}: (6, {}), {1}: (7, {})} | custom-call | tf_op jit(solution)/shard_map/pallas_call | solution.py:360
  (95 shorter events, 3.3 us)
Async XLA Ops:
  0.6 0.8 copy-start
  1.5 7.0 %collective-permute-start.2 = (bf16[128,128]{1,0:T(8,128)(2,1)S(1)}, bf16[128,128]{1,0:T(8,128)(2,1)S(1)}, u32[]{:S(2)}, u32[]{:S(2)}) collective-permute-start(bf16[128,128]{1,0:T(8,128)(2,1)S(1)} %constant_dynamic-slice_fusion), channel_id=1, source_target_pairs={{0,24},{2,26},{4,28},{6,30},{8,16},{10,18},{12,20},{14,22},{16,8},... | collective-permute-start | bytes 98312 | tf_op jit(solution)/shard_map/ppermute | solution.py:21
  6.6 4.8 %collective-permute-start.1 = (bf16[128,128]{1,0:T(8,128)(2,1)S(1)}, bf16[128,128]{1,0:T(8,128)(2,1)S(1)}, u32[]{:S(2)}, u32[]{:S(2)}) collective-permute-start(bf16[128,128]{1,0:T(8,128)(2,1)S(1)} %constant_dynamic-slice_fusion), channel_id=1, source_target_pairs={{0,16},{2,18},{4,20},{6,22},{8,24},{10,26},{12,28},{14,30},{16,0},... | collective-permute-start | bytes 98312 | tf_op jit(solution)/shard_map/ppermute | solution.py:21
  6.6 4.8 %collective-permute-start = (bf16[128,128]{1,0:T(8,128)(2,1)S(1)}, bf16[128,128]{1,0:T(8,128)(2,1)S(1)}, u32[]{:S(2)}, u32[]{:S(2)}) collective-permute-start(bf16[128,128]{1,0:T(8,128)(2,1)S(1)} %constant_dynamic-slice_fusion), channel_id=1, source_target_pairs={{0,8},{2,10},{4,12},{6,14},{8,0},{10,2},{12,4},{14,6},{16,24},{18,... | collective-permute-start | bytes 98312 | tf_op jit(solution)/shard_map/ppermute | solution.py:21
  11.4 6.3 %collective-permute-start.3 = (bf16[512,128]{1,0:T(8,128)(2,1)S(1)}, bf16[512,128]{1,0:T(8,128)(2,1)S(1)}, u32[]{:S(2)}, u32[]{:S(2)}) collective-permute-start(bf16[512,128]{1,0:T(8,128)(2,1)S(1)} %pad_maximum_fusion.refs_0_), channel_id=1, source_target_pairs={{0,2},{2,0},{4,6},{6,4},{8,10},{10,8},{12,14},{14,12},{16,18},{18,... | collective-permute-start | bytes 393224 | tf_op jit(solution)/shard_map/ppermute | solution.py:21
  13.0 5.9 %collective-permute-start.4 = (bf16[512,128]{1,0:T(8,128)(2,1)S(1)}, bf16[512,128]{1,0:T(8,128)(2,1)S(1)}, u32[]{:S(2)}, u32[]{:S(2)}) collective-permute-start(bf16[512,128]{1,0:T(8,128)(2,1)S(1)} %pad_maximum_fusion.refs_0_), channel_id=1, source_target_pairs={{0,4},{2,6},{4,0},{6,2},{8,12},{10,14},{12,8},{14,10},{16,20},{18,... | collective-permute-start | bytes 393224 | tf_op jit(solution)/shard_map/ppermute | solution.py:21
  14.5 5.9 %collective-permute-start.5 = (bf16[512,128]{1,0:T(8,128)(2,1)S(1)}, bf16[512,128]{1,0:T(8,128)(2,1)S(1)}, u32[]{:S(2)}, u32[]{:S(2)}) collective-permute-start(bf16[512,128]{1,0:T(8,128)(2,1)S(1)} %pad_maximum_fusion.refs_0_), channel_id=1, source_target_pairs={{0,6},{2,4},{4,2},{6,0},{8,14},{10,12},{12,10},{14,8},{16,22},{18,... | collective-permute-start | bytes 393224 | tf_op jit(solution)/shard_map/ppermute | solution.py:21
  15.0 5.4 %collective-permute-start.6 = (bf16[512,128]{1,0:T(8,128)(2,1)S(1)}, bf16[512,128]{1,0:T(8,128)(2,1)S(1)}, u32[]{:S(2)}, u32[]{:S(2)}) collective-permute-start(bf16[512,128]{1,0:T(8,128)(2,1)S(1)} %pad_maximum_fusion.refs_0_), channel_id=1, source_target_pairs={{0,1},{1,0},{2,3},{3,2},{4,5},{5,4},{6,7},{7,6},{8,9},{9,8},{10,11... | collective-permute-start | bytes 393224 | tf_op jit(solution)/shard_map/ppermute | solution.py:101
  17.7 2.7 %collective-permute-start.7 = (bf16[512,128]{1,0:T(8,128)(2,1)S(1)}, bf16[512,128]{1,0:T(8,128)(2,1)S(1)}, u32[]{:S(2)}, u32[]{:S(2)}) collective-permute-start(bf16[512,128]{1,0:T(8,128)(2,1)S(1)} %collective-permute-done.3.refs_1_), channel_id=1, source_target_pairs={{0,1},{1,0},{2,3},{3,2},{4,5},{5,4},{6,7},{7,6},{8,9},{9,8},{10,11... | collective-permute-start | bytes 393224 | tf_op jit(solution)/shard_map/ppermute | solution.py:101
  18.9 1.5 collective-permute-start.8
  20.3 1.3 collective-permute-start.9
  28.0 9.0 %collective-permute-start.15 = (bf16[4,16,1536]{2,1,0:T(8,128)(2,1)}, bf16[4,16,1536]{2,1,0:T(8,128)(2,1)S(1)}, u32[]{:S(2)}, u32[]{:S(2)}) collective-permute-start(bf16[4,16,1536]{2,1,0:T(8,128)(2,1)} %get-tuple-element.35), channel_id=1, source_target_pairs={{0,6},{2,4},{4,2},{6,0},{8,14},{10,12},{12,10},{14,8},{16,22},{18,... | collective-permute-start | bytes 589832 | tf_op jit(solution)/shard_map/ppermute | solution.py:21
  28.6 11.1 %collective-permute-start.14 = (bf16[4,16,1536]{2,1,0:T(8,128)(2,1)}, bf16[4,16,1536]{2,1,0:T(8,128)(2,1)S(1)}, u32[]{:S(2)}, u32[]{:S(2)}) collective-permute-start(bf16[4,16,1536]{2,1,0:T(8,128)(2,1)} %get-tuple-element.34), channel_id=1, source_target_pairs={{0,4},{2,6},{4,0},{6,2},{8,12},{10,14},{12,8},{14,10},{16,20},{18,... | collective-permute-start | bytes 589832 | tf_op jit(solution)/shard_map/ppermute | solution.py:21
  30.1 10.2 %collective-permute-start.13 = (bf16[4,16,1536]{2,1,0:T(8,128)(2,1)}, bf16[4,16,1536]{2,1,0:T(8,128)(2,1)S(1)}, u32[]{:S(2)}, u32[]{:S(2)}) collective-permute-start(bf16[4,16,1536]{2,1,0:T(8,128)(2,1)} %get-tuple-element.33), channel_id=1, source_target_pairs={{0,2},{2,0},{4,6},{6,4},{8,10},{10,8},{12,14},{14,12},{16,18},{18,... | collective-permute-start | bytes 589832 | tf_op jit(solution)/shard_map/ppermute | solution.py:21
  41.4 48.4 %copy-start.10 = (f32[16,1024]{1,0:T(8,128)S(1)}, f32[16,1024]{1,0:T(8,128)}, u32[]{:S(2)}) copy-start(f32[16,1024]{1,0:T(8,128)} %first_value.1) | copy-start | bytes 196612
  41.4 48.4 %copy-start.11 = (f32[16,1024]{1,0:T(8,128)S(1)}, f32[16,1024]{1,0:T(8,128)}, u32[]{:S(2)}) copy-start(f32[16,1024]{1,0:T(8,128)} %second_value.1) | copy-start | bytes 196612
  41.4 49.0 %copy-start.12 = (f32[16,512]{1,0:T(8,128)S(1)}, f32[16,512]{1,0:T(8,128)}, u32[]{:S(2)}) copy-start(f32[16,512]{1,0:T(8,128)} %first_key.1) | copy-start | bytes 98308
  41.4 49.0 %copy-start.13 = (f32[16,512]{1,0:T(8,128)S(1)}, f32[16,512]{1,0:T(8,128)}, u32[]{:S(2)}) copy-start(f32[16,512]{1,0:T(8,128)} %second_key.1) | copy-start | bytes 98308
  41.5 6.2 %collective-permute-start.18 = (bf16[16,1536]{1,0:T(8,128)(2,1)S(1)}, bf16[16,1536]{1,0:T(8,128)(2,1)S(1)}, u32[]{:S(2)}, u32[]{:S(2)}) collective-permute-start(bf16[16,1536]{1,0:T(8,128)(2,1)S(1)} %get-tuple-element.57), channel_id=1, source_target_pairs={{0,24},{2,26},{4,28},{6,30},{8,16},{10,18},{12,20},{14,22},{16,8},... | collective-permute-start | bytes 147464 | tf_op jit(solution)/shard_map/ppermute | solution.py:21
  43.3 5.5 %collective-permute-start.17 = (bf16[16,1536]{1,0:T(8,128)(2,1)S(1)}, bf16[16,1536]{1,0:T(8,128)(2,1)S(1)}, u32[]{:S(2)}, u32[]{:S(2)}) collective-permute-start(bf16[16,1536]{1,0:T(8,128)(2,1)S(1)} %get-tuple-element.58), channel_id=1, source_target_pairs={{0,16},{2,18},{4,20},{6,22},{8,24},{10,26},{12,28},{14,30},{16,0},... | collective-permute-start | bytes 147464 | tf_op jit(solution)/shard_map/ppermute | solution.py:21
  43.6 5.2 %collective-permute-start.16 = (bf16[16,1536]{1,0:T(8,128)(2,1)S(1)}, bf16[16,1536]{1,0:T(8,128)(2,1)S(1)}, u32[]{:S(2)}, u32[]{:S(2)}) collective-permute-start(bf16[16,1536]{1,0:T(8,128)(2,1)S(1)} %get-tuple-element.56), channel_id=1, source_target_pairs={{0,8},{2,10},{4,12},{6,14},{8,0},{10,2},{12,4},{14,6},{16,24},{18,... | collective-permute-start | bytes 147464 | tf_op jit(solution)/shard_map/ppermute | solution.py:21
  48.8 6.1 %collective-permute-start.21 = (bf16[16,1536]{1,0:T(8,128)(2,1)S(1)}, bf16[16,1536]{1,0:T(8,128)(2,1)S(1)}, u32[]{:S(2)}, u32[]{:S(2)}) collective-permute-start(bf16[16,1536]{1,0:T(8,128)(2,1)S(1)} %get-tuple-element.50), channel_id=1, source_target_pairs={{0,24},{2,26},{4,28},{6,30},{8,16},{10,18},{12,20},{14,22},{16,8},... | collective-permute-start | bytes 147464 | tf_op jit(solution)/shard_map/ppermute | solution.py:21
  51.3 5.0 %collective-permute-start.20 = (bf16[16,1536]{1,0:T(8,128)(2,1)S(1)}, bf16[16,1536]{1,0:T(8,128)(2,1)S(1)}, u32[]{:S(2)}, u32[]{:S(2)}) collective-permute-start(bf16[16,1536]{1,0:T(8,128)(2,1)S(1)} %get-tuple-element.50), channel_id=1, source_target_pairs={{0,16},{2,18},{4,20},{6,22},{8,24},{10,26},{12,28},{14,30},{16,0},... | collective-permute-start | bytes 147464 | tf_op jit(solution)/shard_map/ppermute | solution.py:21
  51.6 4.8 %collective-permute-start.19 = (bf16[16,1536]{1,0:T(8,128)(2,1)S(1)}, bf16[16,1536]{1,0:T(8,128)(2,1)S(1)}, u32[]{:S(2)}, u32[]{:S(2)}) collective-permute-start(bf16[16,1536]{1,0:T(8,128)(2,1)S(1)} %get-tuple-element.50), channel_id=1, source_target_pairs={{0,8},{2,10},{4,12},{6,14},{8,0},{10,2},{12,4},{14,6},{16,24},{18,... | collective-permute-start | bytes 147464 | tf_op jit(solution)/shard_map/ppermute | solution.py:21
  56.7 8.0 %collective-permute-start.23 = (f32[16,128]{1,0:T(8,128)S(1)}, f32[16,128]{1,0:T(8,128)S(1)}, u32[]{:S(2)}, u32[]{:S(2)}) collective-permute-start(f32[16,128]{1,0:T(8,128)S(1)} %add_add_fusion.1), channel_id=1, source_target_pairs={{0,4},{2,6},{4,0},{6,2},{8,12},{10,14},{12,8},{14,10},{16,20},{18,... | collective-permute-start | bytes 24584 | tf_op jit(solution)/shard_map/ppermute | solution.py:21
  57.7 8.8 %collective-permute-start.24 = (f32[16,128]{1,0:T(8,128)S(1)}, f32[16,128]{1,0:T(8,128)S(1)}, u32[]{:S(2)}, u32[]{:S(2)}) collective-permute-start(f32[16,128]{1,0:T(8,128)S(1)} %add_add_fusion.1), channel_id=1, source_target_pairs={{0,6},{2,4},{4,2},{6,0},{8,14},{10,12},{12,10},{14,8},{16,22},{18,... | collective-permute-start | bytes 24584 | tf_op jit(solution)/shard_map/ppermute | solution.py:21
  59.3 8.4 %collective-permute-start.22 = (f32[16,128]{1,0:T(8,128)S(1)}, f32[16,128]{1,0:T(8,128)S(1)}, u32[]{:S(2)}, u32[]{:S(2)}) collective-permute-start(f32[16,128]{1,0:T(8,128)S(1)} %add_add_fusion.1), channel_id=1, source_target_pairs={{0,2},{2,0},{4,6},{6,4},{8,10},{10,8},{12,14},{14,12},{16,18},{18,... | collective-permute-start | bytes 24584 | tf_op jit(solution)/shard_map/ppermute | solution.py:21
  62.2 7.7 %collective-permute-start.12 = (bf16[16,3072]{1,0:T(8,128)(2,1)}, bf16[16,3072]{1,0:T(8,128)(2,1)S(1)}, u32[]{:S(2)}, u32[]{:S(2)}) collective-permute-start(bf16[16,3072]{1,0:T(8,128)(2,1)} %get-tuple-element.31), channel_id=1, source_target_pairs={{0,24},{2,26},{4,28},{6,30},{8,16},{10,18},{12,20},{14,22},{16,8},... | collective-permute-start | bytes 294920 | tf_op jit(solution)/shard_map/ppermute | solution.py:21
  64.1 8.2 %collective-permute-start.11 = (bf16[16,3072]{1,0:T(8,128)(2,1)}, bf16[16,3072]{1,0:T(8,128)(2,1)S(1)}, u32[]{:S(2)}, u32[]{:S(2)}) collective-permute-start(bf16[16,3072]{1,0:T(8,128)(2,1)} %get-tuple-element.31), channel_id=1, source_target_pairs={{0,16},{2,18},{4,20},{6,22},{8,24},{10,26},{12,28},{14,30},{16,0},... | collective-permute-start | bytes 294920 | tf_op jit(solution)/shard_map/ppermute | solution.py:21
  64.7 8.5 %collective-permute-start.10 = (bf16[16,3072]{1,0:T(8,128)(2,1)}, bf16[16,3072]{1,0:T(8,128)(2,1)S(1)}, u32[]{:S(2)}, u32[]{:S(2)}) collective-permute-start(bf16[16,3072]{1,0:T(8,128)(2,1)} %get-tuple-element.31), channel_id=1, source_target_pairs={{0,8},{2,10},{4,12},{6,14},{8,0},{10,2},{12,4},{14,6},{16,24},{18,... | collective-permute-start | bytes 294920 | tf_op jit(solution)/shard_map/ppermute | solution.py:21
  66.6 48.6 %collective-permute-start.29 = (bf16[128,1536]{1,0:T(8,128)(2,1)}, bf16[128,1536]{1,0:T(8,128)(2,1)S(1)}, u32[]{:S(2)}, u32[]{:S(2)}) collective-permute-start(bf16[128,1536]{1,0:T(8,128)(2,1)} %get-tuple-element.36.refs_2_), channel_id=1, source_target_pairs={{0,2},{2,0},{4,6},{6,4},{8,10},{10,8},{12,14},{14,12},{16,18},{18,... | collective-permute-start | bytes 1179656 | tf_op jit(solution)/shard_map/ppermute | solution.py:21
  67.6 18.4 %collective-permute-start.32 = (bf16[128,1536]{1,0:T(8,128)(2,1)}, bf16[128,1536]{1,0:T(8,128)(2,1)S(1)}, u32[]{:S(2)}, u32[]{:S(2)}) collective-permute-start(bf16[128,1536]{1,0:T(8,128)(2,1)} %get-tuple-element.36.refs_2_), channel_id=1, source_target_pairs={{0,8},{2,10},{4,12},{6,14},{8,0},{10,2},{12,4},{14,6},{16,24},{18,... | collective-permute-start | bytes 1179656 | tf_op jit(solution)/shard_map/ppermute | solution.py:21
  69.9 37.0 %collective-permute-start.30 = (bf16[128,1536]{1,0:T(8,128)(2,1)}, bf16[128,1536]{1,0:T(8,128)(2,1)S(1)}, u32[]{:S(2)}, u32[]{:S(2)}) collective-permute-start(bf16[128,1536]{1,0:T(8,128)(2,1)} %get-tuple-element.36.refs_2_), channel_id=1, source_target_pairs={{0,4},{2,6},{4,0},{6,2},{8,12},{10,14},{12,8},{14,10},{16,20},{18,... | collective-permute-start | bytes 1179656 | tf_op jit(solution)/shard_map/ppermute | solution.py:21
  72.3 35.8 %collective-permute-start.36 = (bf16[128,1536]{1,0:T(8,128)(2,1)}, bf16[128,1536]{1,0:T(8,128)(2,1)}, u32[]{:S(2)}, u32[]{:S(2)}) collective-permute-start(bf16[128,1536]{1,0:T(8,128)(2,1)} %get-tuple-element.36.refs_2_), channel_id=1, source_target_pairs={{0,16},{2,18},{4,20},{6,22},{8,24},{10,26},{12,28},{14,30},{16,0},... | collective-permute-start | bytes 1179656 | tf_op jit(solution)/shard_map/ppermute | solution.py:21
  73.2 13.3 %collective-permute-start.25 = (f32[16,128]{1,0:T(8,128)S(1)}, f32[16,128]{1,0:T(8,128)S(1)}, u32[]{:S(2)}, u32[]{:S(2)}) collective-permute-start(f32[16,128]{1,0:T(8,128)S(1)} %add_add_fusion), channel_id=1, source_target_pairs={{0,1},{1,0},{2,3},{3,2},{4,5},{5,4},{6,7},{7,6},{8,9},{9,8},{10,11... | collective-permute-start | bytes 24584 | tf_op jit(solution)/shard_map/ppermute | solution.py:238
  86.0 68.4 %copy-start.2 = (bf16[128,1536]{1,0:T(8,128)(2,1)}, bf16[128,1536]{1,0:T(8,128)(2,1)S(1)}, u32[]{:S(2)}) copy-start(bf16[128,1536]{1,0:T(8,128)(2,1)S(1)} %collective-permute-done.32.refs_6_) | copy-start | bytes 1179652
  86.0 45.0 %collective-permute-start.33 = (bf16[128,1536]{1,0:T(8,128)(2,1)S(1)}, bf16[128,1536]{1,0:T(8,128)(2,1)}, u32[]{:S(2)}, u32[]{:S(2)}) collective-permute-start(bf16[128,1536]{1,0:T(8,128)(2,1)S(1)} %collective-permute-done.32.refs_6_), channel_id=1, source_target_pairs={{0,2},{2,0},{4,6},{6,4},{8,10},{10,8},{12,14},{14,12},{16,18},{18,... | collective-permute-start | bytes 1179656 | tf_op jit(solution)/shard_map/ppermute | solution.py:21
  88.1 12.2 %collective-permute-start.26 = (bf16[64,1536]{1,0:T(8,128)(2,1)S(1)}, bf16[64,1536]{1,0:T(8,128)(2,1)S(1)}, u32[]{:S(2)}, u32[]{:S(2)}) collective-permute-start(bf16[64,1536]{1,0:T(8,128)(2,1)S(1)} %fusion.1), channel_id=1, source_target_pairs={{0,2},{2,0},{4,6},{6,4},{8,10},{10,8},{12,14},{14,12},{16,18},{18,... | collective-permute-start | bytes 589832 | tf_op jit(solution)/shard_map/ppermute | solution.py:21
  100.3 5.7 %collective-permute-start.27 = (bf16[64,1536]{1,0:T(8,128)(2,1)S(1)}, bf16[64,1536]{1,0:T(8,128)(2,1)S(1)}, u32[]{:S(2)}, u32[]{:S(2)}) collective-permute-start(bf16[64,1536]{1,0:T(8,128)(2,1)S(1)} %fusion.1), channel_id=1, source_target_pairs={{0,4},{2,6},{4,0},{6,2},{8,12},{10,14},{12,8},{14,10},{16,20},{18,... | collective-permute-start | bytes 589832 | tf_op jit(solution)/shard_map/ppermute | solution.py:21
  106.0 8.7 %collective-permute-start.28 = (bf16[64,1536]{1,0:T(8,128)(2,1)S(1)}, bf16[64,1536]{1,0:T(8,128)(2,1)S(1)}, u32[]{:S(2)}, u32[]{:S(2)}) collective-permute-start(bf16[64,1536]{1,0:T(8,128)(2,1)S(1)} %fusion.1), channel_id=1, source_target_pairs={{0,6},{2,4},{4,2},{6,0},{8,14},{10,12},{12,10},{14,8},{16,22},{18,... | collective-permute-start | bytes 589832 | tf_op jit(solution)/shard_map/ppermute | solution.py:21
  106.9 24.1 %copy-start.3 = (bf16[128,1536]{1,0:T(8,128)(2,1)}, bf16[128,1536]{1,0:T(8,128)(2,1)S(1)}, u32[]{:S(2)}) copy-start(bf16[128,1536]{1,0:T(8,128)(2,1)S(1)} %collective-permute-done.30.refs_4_) | copy-start | bytes 1179652
  106.9 25.3 %collective-permute-start.34 = (bf16[128,1536]{1,0:T(8,128)(2,1)S(1)}, bf16[128,1536]{1,0:T(8,128)(2,1)S(1)}, u32[]{:S(2)}, u32[]{:S(2)}) collective-permute-start(bf16[128,1536]{1,0:T(8,128)(2,1)S(1)} %collective-permute-done.32.refs_6_), channel_id=1, source_target_pairs={{0,4},{2,6},{4,0},{6,2},{8,12},{10,14},{12,8},{14,10},{16,20},{18,... | collective-permute-start | bytes 1179656 | tf_op jit(solution)/shard_map/ppermute | solution.py:21
  108.1 14.6 %collective-permute-start.31 = (bf16[128,1536]{1,0:T(8,128)(2,1)S(1)}, bf16[128,1536]{1,0:T(8,128)(2,1)S(1)}, u32[]{:S(2)}, u32[]{:S(2)}) collective-permute-start(bf16[128,1536]{1,0:T(8,128)(2,1)S(1)} %collective-permute-done.30.refs_4_), channel_id=1, source_target_pairs={{0,2},{2,0},{4,6},{6,4},{8,10},{10,8},{12,14},{14,12},{16,18},{18,... | collective-permute-start | bytes 1179656 | tf_op jit(solution)/shard_map/ppermute | solution.py:21
  114.7 19.5 %collective-permute-start.37 = (bf16[128,1536]{1,0:T(8,128)(2,1)}, bf16[128,1536]{1,0:T(8,128)(2,1)S(1)}, u32[]{:S(2)}, u32[]{:S(2)}) collective-permute-start(bf16[128,1536]{1,0:T(8,128)(2,1)} %collective-permute-done.36.refs_10_), channel_id=1, source_target_pairs={{0,2},{2,0},{4,6},{6,4},{8,10},{10,8},{12,14},{14,12},{16,18},{18,... | collective-permute-start | bytes 1179656 | tf_op jit(solution)/shard_map/ppermute | solution.py:21
  115.2 39.2 %copy-start.1 = (bf16[128,1536]{1,0:T(8,128)(2,1)}, bf16[128,1536]{1,0:T(8,128)(2,1)S(1)}, u32[]{:S(2)}) copy-start(bf16[128,1536]{1,0:T(8,128)(2,1)S(1)} %collective-permute-done.29.refs_3_) | copy-start | bytes 1179652
  115.2 20.0 %collective-permute-start.38 = (bf16[128,1536]{1,0:T(8,128)(2,1)}, bf16[128,1536]{1,0:T(8,128)(2,1)S(1)}, u32[]{:S(2)}, u32[]{:S(2)}) collective-permute-start(bf16[128,1536]{1,0:T(8,128)(2,1)} %collective-permute-done.36.refs_10_), channel_id=1, source_target_pairs={{0,4},{2,6},{4,0},{6,2},{8,12},{10,14},{12,8},{14,10},{16,20},{18,... | collective-permute-start | bytes 1179656 | tf_op jit(solution)/shard_map/ppermute | solution.py:21
  122.7 30.2 %copy-start.5 = (bf16[128,1536]{1,0:T(8,128)(2,1)}, bf16[128,1536]{1,0:T(8,128)(2,1)S(1)}, u32[]{:S(2)}) copy-start(bf16[128,1536]{1,0:T(8,128)(2,1)S(1)} %collective-permute-done.31.refs_5_) | copy-start | bytes 1179652
  122.7 8.0 %collective-permute-start.40 = (bf16[128,1536]{1,0:T(8,128)(2,1)}, bf16[128,1536]{1,0:T(8,128)(2,1)S(1)}, u32[]{:S(2)}, u32[]{:S(2)}) collective-permute-start(bf16[128,1536]{1,0:T(8,128)(2,1)} %collective-permute-done.36.refs_10_), channel_id=1, source_target_pairs={{0,8},{2,10},{4,12},{6,14},{8,0},{10,2},{12,4},{14,6},{16,24},{18,... | collective-permute-start | bytes 1179656 | tf_op jit(solution)/shard_map/ppermute | solution.py:21
  130.7 31.8 %collective-permute-start.41 = (bf16[128,1536]{1,0:T(8,128)(2,1)S(1)}, bf16[128,1536]{1,0:T(8,128)(2,1)S(1)}, u32[]{:S(2)}, u32[]{:S(2)}) collective-permute-start(bf16[128,1536]{1,0:T(8,128)(2,1)S(1)} %collective-permute-done.40.refs_2_), channel_id=1, source_target_pairs={{0,2},{2,0},{4,6},{6,4},{8,10},{10,8},{12,14},{14,12},{16,18},{18,... | collective-permute-start | bytes 1179656 | tf_op jit(solution)/shard_map/ppermute | solution.py:21
  131.0 31.5 %collective-permute-start.42 = (bf16[128,1536]{1,0:T(8,128)(2,1)S(1)}, bf16[128,1536]{1,0:T(8,128)(2,1)S(1)}, u32[]{:S(2)}, u32[]{:S(2)}) collective-permute-start(bf16[128,1536]{1,0:T(8,128)(2,1)S(1)} %collective-permute-done.40.refs_2_), channel_id=1, source_target_pairs={{0,4},{2,6},{4,0},{6,2},{8,12},{10,14},{12,8},{14,10},{16,20},{18,... | collective-permute-start | bytes 1179656 | tf_op jit(solution)/shard_map/ppermute | solution.py:21
  132.1 3.5 %copy-start.4 = (bf16[128,1536]{1,0:T(8,128)(2,1)}, bf16[128,1536]{1,0:T(8,128)(2,1)S(1)}, u32[]{:S(2)}) copy-start(bf16[128,1536]{1,0:T(8,128)(2,1)S(1)} %collective-permute-done.34.refs_8_) | copy-start | bytes 1179652
  132.1 30.3 %collective-permute-start.43 = (bf16[128,1536]{1,0:T(8,128)(2,1)S(1)}, bf16[128,1536]{1,0:T(8,128)(2,1)S(1)}, u32[]{:S(2)}, u32[]{:S(2)}) collective-permute-start(bf16[128,1536]{1,0:T(8,128)(2,1)S(1)} %collective-permute-done.40.refs_2_), channel_id=1, source_target_pairs={{0,6},{2,4},{4,2},{6,0},{8,14},{10,12},{12,10},{14,8},{16,22},{18,... | collective-permute-start | bytes 1179656 | tf_op jit(solution)/shard_map/ppermute | solution.py:21
  134.2 18.7 %copy-start.6 = (bf16[128,1536]{1,0:T(8,128)(2,1)}, bf16[128,1536]{1,0:T(8,128)(2,1)S(1)}, u32[]{:S(2)}) copy-start(bf16[128,1536]{1,0:T(8,128)(2,1)S(1)} %collective-permute-done.37.refs_11_) | copy-start | bytes 1179652
  134.2 18.7 %collective-permute-start.35 = (bf16[128,1536]{1,0:T(8,128)(2,1)}, bf16[128,1536]{1,0:T(8,128)(2,1)S(1)}, u32[]{:S(2)}, u32[]{:S(2)}) collective-permute-start(bf16[128,1536]{1,0:T(8,128)(2,1)} %collective-permute-done.33.refs_7_), channel_id=1, source_target_pairs={{0,4},{2,6},{4,0},{6,2},{8,12},{10,14},{12,8},{14,10},{16,20},{18,... | collective-permute-start | bytes 1179656 | tf_op jit(solution)/shard_map/ppermute | solution.py:21
  135.2 17.7 %copy-start.7 = (bf16[128,1536]{1,0:T(8,128)(2,1)}, bf16[128,1536]{1,0:T(8,128)(2,1)S(1)}, u32[]{:S(2)}) copy-start(bf16[128,1536]{1,0:T(8,128)(2,1)S(1)} %collective-permute-done.38.refs_12_) | copy-start | bytes 1179652
  135.2 17.7 %collective-permute-start.39 = (bf16[128,1536]{1,0:T(8,128)(2,1)S(1)}, bf16[128,1536]{1,0:T(8,128)(2,1)S(1)}, u32[]{:S(2)}, u32[]{:S(2)}) collective-permute-start(bf16[128,1536]{1,0:T(8,128)(2,1)S(1)} %collective-permute-done.38.refs_12_), channel_id=1, source_target_pairs={{0,2},{2,0},{4,6},{6,4},{8,10},{10,8},{12,14},{14,12},{16,18},{18,... | collective-permute-start | bytes 1179656 | tf_op jit(solution)/shard_map/ppermute | solution.py:21
  152.9 0.8 copy-start.8
  153.6 0.8 copy-start.9

commit v3 on v2

--- a/solution.py
+++ b/solution.py
@@ -53,11 +53,12 @@
         first = swap(shard, ranks, 1)
         second = swap(shard, ranks, 2)
         if chunk == last:
-            third = swap(shard, ranks, 3)
-        elif chunk % 2:
-            third = swap(first, ranks, 2)
-        else:
-            third = swap(second, ranks, 1)
+            half = shard.shape[0] // 2
+            top = swap(second[:half], ranks, 1)
+            bottom = swap(first[half:], ranks, 2)
+            chunks.append((chunk, [(0, 0, shard), (1, 0, first), (2, 0, second), (3, 0, top), (3, half, bottom)]))
+            continue
+        third = swap(first, ranks, 2) if chunk % 2 else swap(second, ranks, 1)
         chunks.append((chunk, [(away, 0, part) for away, part in enumerate((shard, first, second, third))]))
     return chunks
 
@@ -239,7 +240,7 @@
     return jnp.sum(total)
 
 
-def copy_kernel(layout, with_own, inherited, *refs):
+def copy_kernel(layout, with_own, inherited, resident, *refs):
     count = sum(len(parts) for _, parts in layout)
     basis, directions, *rest = refs
     pieces, rest = rest[:count], rest[count:]
@@ -247,14 +248,14 @@
     rest = rest[inherited:]
     copy_key, copy_value, *rest = rest
     results, rest = (rest[:4], rest[4:]) if with_own else ((), rest)
-    taken, made, step, take_sem, key_sem, value_sem, *rest = rest
+    taken, made, step, take_sem, copy_sem, *rest = rest
     rows = step.shape[0] // INNER
     key_cols = copy_key.shape[1]
     here = lax.axis_index("fs")
     inner = here % INNER
     outer = here // INNER
     takes = []
-    if with_own:
+    if not resident:
         takes = [
             pltpu.make_async_copy(piece, taken.at[slot, pl.ds(0, piece.shape[0])], take_sem.at[slot])
             for slot, piece in enumerate(pieces)
@@ -271,45 +272,46 @@
             take.start()
     gives = []
     slot = 0
+    blocks = step.shape[1] // key_cols
     for chunk, parts in layout:
         first_row = pl.multiple_of((outer ^ chunk) * INNER * rows, INNER * rows)
-        if len(parts) == INNER:
-            step[...] = jnp.dot(
-                basis[pl.ds(first_row, INNER * rows), :], directions[...], preferred_element_type=jnp.float32
+        own_spot = pl.ds(pl.multiple_of(inner * rows, rows), rows)
+        if with_own and chunk == 0:
+            for take in own_takes:
+                take.wait()
+        for block in range(blocks):
+            columns = pl.ds(block * key_cols, key_cols)
+            step[:, columns] = jnp.dot(
+                basis[pl.ds(first_row, INNER * rows), :], directions[:, columns], preferred_element_type=jnp.float32
             )
-        for away, start in parts:
-            size = pieces[slot].shape[0]
-            spot = pl.multiple_of((inner ^ away) * rows + start, size)
-            if len(parts) != INNER:
-                step[pl.ds(spot, size), :] = jnp.dot(
-                    basis[pl.ds(pl.multiple_of(first_row + spot, size), size), :],
-                    directions[...],
-                    preferred_element_type=jnp.float32,
-                )
-            if takes:
-                takes[slot].wait()
-                piece = taken[slot, pl.ds(0, size)]
-            else:
-                piece = pieces[slot][...]
-            change = learn_rate * step[pl.ds(spot, size), :]
-            made[slot, pl.ds(0, size)] = (piece.astype(jnp.float32) - change).astype(jnp.bfloat16)
-            target = pl.ds(pl.multiple_of(first_row + spot, size), size)
-            for out_ref, columns, sem in (
-                (copy_key, pl.ds(0, key_cols), key_sem),
-                (copy_value, pl.ds(key_cols, step.shape[1] - key_cols), value_sem),
-            ):
+            for index, (away, start) in enumerate(parts, slot):
+                size = pieces[index].shape[0]
+                spot = pl.multiple_of((inner ^ away) * rows + start, size)
+                if takes:
+                    if block == 0:
+                        takes[index].wait()
+                    piece = taken[index, pl.ds(0, size), columns]
+                else:
+                    piece = pieces[index][:, columns]
+                change = learn_rate * step[pl.ds(spot, size), columns]
+                made[index, pl.ds(0, size), columns] = (piece.astype(jnp.float32) - change).astype(jnp.bfloat16)
+                target = pl.ds(pl.multiple_of(first_row + spot, size), size)
+                goal = copy_value.at[target, pl.ds((block - 1) * key_cols, key_cols)] if block else copy_key.at[target, :]
                 give = pltpu.make_async_copy(
-                    made.at[slot, pl.ds(0, size), columns], out_ref.at[target, :], sem.at[slot]
+                    made.at[index, pl.ds(0, size), columns], goal, copy_sem.at[index, block]
                 )
                 give.start()
                 gives.append(give)
-            slot += 1
+            if with_own and chunk == 0:
+                change = step[own_spot, columns]
+                own_step[:, columns] = change
+                if block:
+                    part = pl.ds((block - 1) * key_cols, key_cols)
+                    own_value[:, part] = own_value[:, part] - learn_rate * change
+                else:
+                    own_key[...] = own_key[...] - learn_rate * change
+        slot += len(parts)
         if with_own and chunk == 0:
-            for take in own_takes:
-                take.wait()
-            own_step[...] = step[pl.ds(pl.multiple_of(inner * rows, rows), rows), :]
-            own_key[...] = own_key[...] - learn_rate * own_step[:, :key_cols]
-            own_value[...] = own_value[...] - learn_rate * own_step[:, key_cols:]
             value_cols = step.shape[1] - key_cols
             for place_in, (source, target) in enumerate(
                 (
@@ -326,7 +328,7 @@
         give.wait()
 
 
-def write_copies(chunks, masters, basis, directions, key_cols, ranks, earlier):
+def write_copies(chunks, masters, basis, directions, key_cols, ranks, earlier, resident):
     rows = basis.shape[0] // ranks
     cols = directions.shape[1]
     layout = tuple((chunk, tuple((away, start) for away, start, _ in parts)) for chunk, parts in chunks)
@@ -344,8 +346,7 @@
         pltpu.VMEM((count, tallest, cols), jnp.bfloat16),
         pltpu.VMEM((INNER * rows, cols), jnp.float32),
         pltpu.SemaphoreType.DMA((count,)),
-        pltpu.SemaphoreType.DMA((count,)),
-        pltpu.SemaphoreType.DMA((count,)),
+        pltpu.SemaphoreType.DMA((count, cols // key_cols)),
     ]
     if masters:
         out_shape += [jax.ShapeDtypeStruct(master.shape, jnp.float32) for master in (*masters, *masters)]
@@ -358,15 +359,15 @@
         ]
     first_alias = 2 + count + len(masters)
     return pl.pallas_call(
-        functools.partial(copy_kernel, layout, bool(masters), len(earlier)),
+        functools.partial(copy_kernel, layout, bool(masters), len(earlier), resident),
         in_specs=[local, local]
-        + [anywhere if masters else local] * count
+        + [local if resident else anywhere] * count
         + [anywhere] * (len(masters) + len(earlier)),
         out_specs=[anywhere] * len(out_shape),
         out_shape=out_shape,
         scratch_shapes=scratch,
         input_output_aliases={first_alias: 0, first_alias + 1: 1} if earlier else {},
-    )(basis, *in_vmem(directions), *(pieces if masters else in_vmem(*pieces)), *masters, *earlier)
+    )(basis, *in_vmem(directions), *(in_vmem(*pieces) if resident else pieces), *masters, *earlier)
 
 
 def on_device(
@@ -414,11 +415,12 @@
     new_first_key, new_second_key = advance(low[:, :key_cols], first_key, second_key)
     new_first_value, new_second_value = advance(low[:, key_cols:], first_value, second_value)
     copy_key, copy_value, *own = write_copies(
-        chunks[:-1], (master_key, master_value), whole_basis, directions, key_cols, ranks, ()
+        chunks[:-2], (master_key, master_value), whole_basis, directions, key_cols, ranks, (), False
     )
-    copy_key, copy_value = write_copies(
-        chunks[-1:], (), whole_basis, directions, key_cols, ranks, (copy_key, copy_value)
-    )
+    for name, some in (("middle", chunks[-2:-1]), ("late", chunks[-1:])):
+        copy_key, copy_value = write_copies(
+            some, (), whole_basis, directions, key_cols, ranks, (copy_key, copy_value), name == "late"
+        )
     return (*own, copy_key, copy_value, new_first_key, new_second_key, new_first_value, new_second_value)
 
 

time: 166 us -> 160 us (0.964)
  waiting for transfers between devices: 91.7 us -> 83.6 us
  Pallas kernels: 19.6 us -> 22.4 us
    ppermute x39 -> x40, waiting for transfers between devices: 90.3 us -> 82.3 us  [swap(): lax.ppermute(values, 'fs', [(rank, rank ^ offset) for rank in range(ranks)])]
    pallas_call x2 -> x3, Pallas kernels: 11.4 us -> 14.1 us  [write_copies(): pl.pallas_call(functools.partial(copy_kernel, layout, bool(masters), len(...]
    ppermute x39 -> x40, starting transfers between devices: 45.7 us -> 44.3 us  [swap(): lax.ppermute(values, 'fs', [(rank, rank ^ offset) for rank in range(ranks)])]
  transfers between devices with their start and end apart: 44 -> 45, of which waited for: 22 -> 20; matrix products, arithmetic and copies ran while one was open for 2% -> 3% of each run, Pallas kernels for 6% -> 8%
where the time goes in v3:
time: 160 us
  waiting for transfers between devices  83.6 us (52%)
  starting transfers between devices  44.4 us (28%)
  Pallas kernels  22.4 us (14%)
  other arithmetic  4.39 us (3%)
  local copies, waits for them, and re-layouts  3.34 us (2%)
  between operations  1.78 us (1%)
    ppermute x40, waiting for transfers between devices, swap(): lax.ppermute(values, 'fs', [(rank, rank ^ offset) for rank in range(ranks)])  82.3 us
    ppermute x40, starting transfers between devices, swap(): lax.ppermute(values, 'fs', [(rank, rank ^ offset) for rank in range(ranks)])  44.3 us
    pallas_call x3, Pallas kernels, write_copies(): pl.pallas_call(functools.partial(copy_kernel, layout, bool(masters), len(...  14.1 us
    pallas_call x1, Pallas kernels, project(): pl.pallas_call(functools.partial(project_kernel, groups), in_specs=[local...  6.31 us
  transfers between devices with their start and end apart: 45, of which 20 were waited for; matrix products, arithmetic and copies ran while one was open for 3% of the time, Pallas kernels for 8%

profile of v3, /device:TPU:0, one launch (start us, length us, event | category | flops | bytes accessed | tf_op | source)
XLA Modules:
  0.0 159.8 jit_solution(5306817982135633517)
XLA Ops:
  0.7 0.8 copy-done
  1.5 3.1 %collective-permute-start = (bf16[128,128]{1,0:T(8,128)(2,1)S(1)}, bf16[128,128]{1,0:T(8,128)(2,1)S(1)}, u32[]{:S(2)}, u32[]{:S(2)}) collective-permute-start(bf16[128,128]{1,0:T(8,128)(2,1)S(1)} %constant_dynamic-slice_fusion), channel_id=1, source_target_pairs={{0,8},{2,10},{4,12},{6,14},{8,0},{10,2},{12,4},{14,6},{16,24},{18,... | collective-permute-start | bytes 98312 | tf_op jit(solution)/shard_map/ppermute | solution.py:21
  4.5 2.6 %collective-permute-start.1 = (bf16[128,128]{1,0:T(8,128)(2,1)S(1)}, bf16[128,128]{1,0:T(8,128)(2,1)S(1)}, u32[]{:S(2)}, u32[]{:S(2)}) collective-permute-start(bf16[128,128]{1,0:T(8,128)(2,1)S(1)} %constant_dynamic-slice_fusion), channel_id=1, source_target_pairs={{0,16},{2,18},{4,20},{6,22},{8,24},{10,26},{12,28},{14,30},{16,0},... | collective-permute-start | bytes 98312 | tf_op jit(solution)/shard_map/ppermute | solution.py:21
  7.1 2.8 %collective-permute-done.1 = bf16[128,128]{1,0:T(8,128)(2,1)S(1)} collective-permute-done((bf16[128,128]{1,0:T(8,128)(2,1)S(1)}, bf16[128,128]{1,0:T(8,128)(2,1)S(1)}, u32[]{:S(2)}, u32[]{:S(2)}) %collective-permute-start.1) | collective-permute-done | bytes 32800 | tf_op jit(solution)/shard_map/ppermute | solution.py:21
  9.9 2.9 %collective-permute-done.2 = bf16[128,128]{1,0:T(8,128)(2,1)S(1)} collective-permute-done((bf16[128,128]{1,0:T(8,128)(2,1)S(1)}, bf16[128,128]{1,0:T(8,128)(2,1)S(1)}, u32[]{:S(2)}, u32[]{:S(2)}) %collective-permute-start.2) | collective-permute-done | bytes 32800 | tf_op jit(solution)/shard_map/ppermute | solution.py:21
  12.9 1.6 collective-permute-start.3
  14.4 1.5 collective-permute-start.4
  15.9 0.5 collective-permute-start.5
  16.4 2.5 %collective-permute-done.3.refs_1_ = bf16[512,128]{1,0:T(8,128)(2,1)S(1)} collective-permute-done((bf16[512,128]{1,0:T(8,128)(2,1)S(1)}, bf16[512,128]{1,0:T(8,128)(2,1)S(1)}, u32[]{:S(2)}, u32[]{:S(2)}) %collective-permute-start.3) | collective-permute-done | bytes 131104 | tf_op jit(solution)/shard_map/ppermute | solution.py:21
  19.0 1.2 collective-permute-done.4.refs_2_
  20.2 1.6 %collective-permute-done.5.refs_3_ = bf16[512,128]{1,0:T(8,128)(2,1)S(1)} collective-permute-done((bf16[512,128]{1,0:T(8,128)(2,1)S(1)}, bf16[512,128]{1,0:T(8,128)(2,1)S(1)}, u32[]{:S(2)}, u32[]{:S(2)}) %collective-permute-start.5) | collective-permute-done | bytes 131104 | tf_op jit(solution)/shard_map/ppermute | solution.py:21
  21.8 1.3 collective-permute-done.9.refs_7_
  23.2 6.3 %project.1 = (bf16[2048,256]{1,0:T(8,128)(2,1)}, f32[4,16,1536]{2,1,0:T(8,128)}, bf16[4,16,1536]{2,1,0:T(8,128)(2,1)}, bf16[4,16,1536]{2,1,0:T(8,128)(2,1)}, bf16[4,16,1536]{2,1,0:T(8,128)(2,1)}) custom-call(bf16[512,128]{1,0:T(8,128)(2,1)S(1)} %pad_maximum_fusion.refs_0_, bf16[512,128]{1,0:T(8,128)(2,1)S(1)} %collective-permute-done.3.refs_1_, ...), custom_call_target="tpu_custom_call" | custom-call | tf_op jit(solution)/shard_map/project/pallas_call | solution.py:184
  29.5 0.6 collective-permute-start.13
  30.1 0.5 collective-permute-start.14
  30.6 2.4 %collective-permute-start.15 = (bf16[4,16,1536]{2,1,0:T(8,128)(2,1)}, bf16[4,16,1536]{2,1,0:T(8,128)(2,1)S(1)}, u32[]{:S(2)}, u32[]{:S(2)}) collective-permute-start(bf16[4,16,1536]{2,1,0:T(8,128)(2,1)} %get-tuple-element.37), channel_id=1, source_target_pairs={{0,6},{2,4},{4,2},{6,0},{8,14},{10,12},{12,10},{14,8},{16,22},{18,... | collective-permute-start | bytes 589832 | tf_op jit(solution)/shard_map/ppermute | solution.py:21
  33.0 4.5 %collective-permute-done.13 = bf16[4,16,1536]{2,1,0:T(8,128)(2,1)S(1)} collective-permute-done((bf16[4,16,1536]{2,1,0:T(8,128)(2,1)}, bf16[4,16,1536]{2,1,0:T(8,128)(2,1)S(1)}, u32[]{:S(2)}, u32[]{:S(2)}) %collective-permute-start.13) | collective-permute-done | bytes 196640 | tf_op jit(solution)/shard_map/ppermute | solution.py:21
  37.5 4.0 %collective-permute-done.15 = bf16[4,16,1536]{2,1,0:T(8,128)(2,1)S(1)} collective-permute-done((bf16[4,16,1536]{2,1,0:T(8,128)(2,1)}, bf16[4,16,1536]{2,1,0:T(8,128)(2,1)S(1)}, u32[]{:S(2)}, u32[]{:S(2)}) %collective-permute-start.15) | collective-permute-done | bytes 196640 | tf_op jit(solution)/shard_map/ppermute | solution.py:21
  41.5 1.1 convert_add_fusion
  42.8 1.1 collective-permute-start.17
  43.9 3.3 %collective-permute-start.18 = (bf16[16,1536]{1,0:T(8,128)(2,1)S(1)}, bf16[16,1536]{1,0:T(8,128)(2,1)S(1)}, u32[]{:S(2)}, u32[]{:S(2)}) collective-permute-start(bf16[16,1536]{1,0:T(8,128)(2,1)S(1)} %get-tuple-element.61), channel_id=1, source_target_pairs={{0,24},{2,26},{4,28},{6,30},{8,16},{10,18},{12,20},{14,22},{16,8},... | collective-permute-start | bytes 147464 | tf_op jit(solution)/shard_map/ppermute | solution.py:21
  47.1 1.4 collective-permute-done.17
  48.5 1.3 collective-permute-done.18
  49.9 0.9 collective-permute-start.19
  50.7 3.3 %collective-permute-start.20 = (bf16[16,1536]{1,0:T(8,128)(2,1)S(1)}, bf16[16,1536]{1,0:T(8,128)(2,1)S(1)}, u32[]{:S(2)}, u32[]{:S(2)}) collective-permute-start(bf16[16,1536]{1,0:T(8,128)(2,1)S(1)} %get-tuple-element.54), channel_id=1, source_target_pairs={{0,16},{2,18},{4,20},{6,22},{8,24},{10,26},{12,28},{14,30},{16,0},... | collective-permute-start | bytes 147464 | tf_op jit(solution)/shard_map/ppermute | solution.py:21
  54.3 2.8 %collective-permute-done.20 = bf16[16,1536]{1,0:T(8,128)(2,1)S(1)} collective-permute-done((bf16[16,1536]{1,0:T(8,128)(2,1)S(1)}, bf16[16,1536]{1,0:T(8,128)(2,1)S(1)}, u32[]{:S(2)}, u32[]{:S(2)}) %collective-permute-start.20) | collective-permute-done | bytes 49184 | tf_op jit(solution)/shard_map/ppermute | solution.py:21
  57.1 2.9 %collective-permute-done.21 = bf16[16,1536]{1,0:T(8,128)(2,1)S(1)} collective-permute-done((bf16[16,1536]{1,0:T(8,128)(2,1)S(1)}, bf16[16,1536]{1,0:T(8,128)(2,1)S(1)}, u32[]{:S(2)}, u32[]{:S(2)}) %collective-permute-start.21) | collective-permute-done | bytes 49184 | tf_op jit(solution)/shard_map/ppermute | solution.py:21
  60.3 0.8 collective-permute-start.22
  61.1 1.2 collective-permute-start.23
  62.4 1.5 collective-permute-start.24
  63.9 1.9 %prepare.1 = (bf16[128,1536]{1,0:T(8,128)(2,1)}, bf16[16,3072]{1,0:T(8,128)(2,1)}) custom-call(f32[128,512]{1,0:T(8,128)} %refs_10_.3, f32[128,1024]{1,0:T(8,128)} %refs_11_.1, f32[16,512]{1,0:T(8,128)} %first_key.1, f32[16,512]{1,0:T(8,128)} %second_key.1, f32[16,1024]{1,0:T(8,128)} %first_value.1, f32[16,1024]{1,0:T(8,128)} %second_value.1), custom_call_target="tpu_custom_call" | custom-call | tf_op jit(solution)/shard_map/prepare/pallas_call | solution.py:83
  65.8 1.1 collective-permute-start.11
  66.9 3.3 %collective-permute-start.12 = (bf16[16,3072]{1,0:T(8,128)(2,1)}, bf16[16,3072]{1,0:T(8,128)(2,1)S(1)}, u32[]{:S(2)}, u32[]{:S(2)}) collective-permute-start(bf16[16,3072]{1,0:T(8,128)(2,1)} %get-tuple-element.33), channel_id=1, source_target_pairs={{0,24},{2,26},{4,28},{6,30},{8,16},{10,18},{12,20},{14,22},{16,8},... | collective-permute-start | bytes 294920 | tf_op jit(solution)/shard_map/ppermute | solution.py:21
  70.2 1.1 collective-permute-start.36
  71.3 5.0 %collective-permute-done.10 = bf16[16,3072]{1,0:T(8,128)(2,1)S(1)} collective-permute-done((bf16[16,3072]{1,0:T(8,128)(2,1)}, bf16[16,3072]{1,0:T(8,128)(2,1)S(1)}, u32[]{:S(2)}, u32[]{:S(2)}) %collective-permute-start.10) | collective-permute-done | bytes 98336 | tf_op jit(solution)/shard_map/ppermute | solution.py:21
  76.3 0.8 collective-permute-start.30
  77.1 0.7 collective-permute-start.29
  77.8 0.9 maximum_convert_fusion
  78.7 7.7 %collective-permute-done.32.refs_6_ = bf16[128,1536]{1,0:T(8,128)(2,1)S(1)} collective-permute-done((bf16[128,1536]{1,0:T(8,128)(2,1)}, bf16[128,1536]{1,0:T(8,128)(2,1)S(1)}, u32[]{:S(2)}, u32[]{:S(2)}) %collective-permute-start.32) | collective-permute-done | bytes 393248 | tf_op jit(solution)/shard_map/ppermute | solution.py:21
  86.5 0.6 collective-permute-start.33
  87.0 3.5 %collective-permute-done.36.refs_2_ = bf16[128,1536]{1,0:T(8,128)(2,1)} collective-permute-done((bf16[128,1536]{1,0:T(8,128)(2,1)}, bf16[128,1536]{1,0:T(8,128)(2,1)}, u32[]{:S(2)}, u32[]{:S(2)}) %collective-permute-start.36) | collective-permute-done | bytes 393248 | tf_op jit(solution)/shard_map/ppermute | solution.py:21
  90.6 0.6 add_reduce_fusion
  92.1 0.6 collective-permute-start.26
  92.9 0.7 fusion.7
  93.5 0.6 fusion.11
  94.2 5.7 %collective-permute-done.26 = bf16[64,1536]{1,0:T(8,128)(2,1)S(1)} collective-permute-done((bf16[64,1536]{1,0:T(8,128)(2,1)S(1)}, bf16[64,1536]{1,0:T(8,128)(2,1)S(1)}, u32[]{:S(2)}, u32[]{:S(2)}) %collective-permute-start.26) | collective-permute-done | bytes 196640 | tf_op jit(solution)/shard_map/ppermute | solution.py:21
  99.9 0.7 collective-permute-start.27
  100.7 1.4 collective-permute-start.28
  102.1 7.2 %collective-permute-done.27 = bf16[64,1536]{1,0:T(8,128)(2,1)S(1)} collective-permute-done((bf16[64,1536]{1,0:T(8,128)(2,1)S(1)}, bf16[64,1536]{1,0:T(8,128)(2,1)S(1)}, u32[]{:S(2)}, u32[]{:S(2)}) %collective-permute-start.27) | collective-permute-done | bytes 196640 | tf_op jit(solution)/shard_map/ppermute | solution.py:21
  109.5 0.8 collective-permute-start.38
  110.3 1.7 %collective-permute-start.34 = (bf16[128,1536]{1,0:T(8,128)(2,1)S(1)}, bf16[128,1536]{1,0:T(8,128)(2,1)S(1)}, u32[]{:S(2)}, u32[]{:S(2)}) collective-permute-start(bf16[128,1536]{1,0:T(8,128)(2,1)S(1)} %collective-permute-done.32.refs_6_), channel_id=1, source_target_pairs={{0,4},{2,6},{4,0},{6,2},{8,12},{10,14},{12,8},{14,10},{16,20},{18,... | collective-permute-start | bytes 1179656 | tf_op jit(solution)/shard_map/ppermute | solution.py:21
  112.0 9.3 %collective-permute-done.39.refs_4_ = bf16[128,1536]{1,0:T(8,128)(2,1)S(1)} collective-permute-done((bf16[128,1536]{1,0:T(8,128)(2,1)S(1)}, bf16[128,1536]{1,0:T(8,128)(2,1)S(1)}, u32[]{:S(2)}, u32[]{:S(2)}) %collective-permute-start.39) | collective-permute-done | bytes 393248 | tf_op jit(solution)/shard_map/ppermute | solution.py:21
  121.4 0.7 collective-permute-start.31
  122.2 0.7 slice.126
  122.9 1.3 collective-permute-start.42
  124.2 1.9 %collective-permute-start.35 = (bf16[128,1536]{1,0:T(8,128)(2,1)}, bf16[128,1536]{1,0:T(8,128)(2,1)S(1)}, u32[]{:S(2)}, u32[]{:S(2)}) collective-permute-start(bf16[128,1536]{1,0:T(8,128)(2,1)} %collective-permute-done.33.refs_7_), channel_id=1, source_target_pairs={{0,4},{2,6},{4,0},{6,2},{8,12},{10,14},{12,8},{14,10},{16,20},{18,... | collective-permute-start | bytes 1179656 | tf_op jit(solution)/shard_map/ppermute | solution.py:21
  126.1 12.0 %collective-permute-done.43.refs_4_ = bf16[128,1536]{1,0:T(8,128)(2,1)S(1)} collective-permute-done((bf16[128,1536]{1,0:T(8,128)(2,1)}, bf16[128,1536]{1,0:T(8,128)(2,1)S(1)}, u32[]{:S(2)}, u32[]{:S(2)}) %collective-permute-start.43) | collective-permute-done | bytes 393248 | tf_op jit(solution)/shard_map/ppermute | solution.py:21
  138.6 1.6 %collective-permute-start.40 = (bf16[64,1536]{1,0:T(8,128)(2,1)}, bf16[64,1536]{1,0:T(8,128)(2,1)S(1)}, u32[]{:S(2)}, u32[]{:S(2)}) collective-permute-start(bf16[64,1536]{1,0:T(8,128)(2,1)} %slice.126), channel_id=1, source_target_pairs={{0,2},{2,0},{4,6},{6,4},{8,10},{10,8},{12,14},{14,12},{16,18},{18,... | collective-permute-start | bytes 589832 | tf_op jit(solution)/shard_map/ppermute | solution.py:21
  140.4 3.8 %collective-permute-done.35.refs_9_ = bf16[128,1536]{1,0:T(8,128)(2,1)S(1)} collective-permute-done((bf16[128,1536]{1,0:T(8,128)(2,1)}, bf16[128,1536]{1,0:T(8,128)(2,1)S(1)}, u32[]{:S(2)}, u32[]{:S(2)}) %collective-permute-start.35) | collective-permute-done | bytes 393248 | tf_op jit(solution)/shard_map/ppermute | solution.py:21
  144.2 0.7 copy-done.6
  144.9 6.7 %shard_map.177 = (bf16[2048,512]{1,0:T(8,128)(2,1)}, bf16[2048,1024]{1,0:T(8,128)(2,1)}, f32[128,512]{1,0:T(8,128)}, f32[128,1024]{1,0:T(8,128)}, f32[128,512]{1,0:T(8,128)}, /*index=5*/f32[128,1024]{1,0:T(8,128)}) custom-call(bf16[2048,256]{1,0:T(8,128)(2,1)} %get-tuple-element.32.refs_0_, bf16[256,1536]{1,0:T(8,128)(2,1)S(1)} %slice_dynamic-update-slice_fusion.refs_1_, ...), custom_call_target="tpu_custom_call" | custom-call | tf_op jit(solution)/shard_map/pallas_call | solution.py:361
  151.7 0.7 copy-done.2
  152.4 4.2 %shard_map.178 = (bf16[2048,512]{1,0:T(8,128)(2,1)}, bf16[2048,1024]{1,0:T(8,128)(2,1)}) custom-call(bf16[2048,256]{1,0:T(8,128)(2,1)} %get-tuple-element.32.refs_0_, bf16[256,1536]{1,0:T(8,128)(2,1)S(1)} %slice_dynamic-update-slice_fusion.refs_1_, bf16[128,1536]{1,0:T(8,128)(2,1)} %collective-permute-done.36.refs_2_, ...), custom_call_target="tpu_custom_call", output_to_operand_aliasing={{0}: (6, {}), {1}: (7, {})} | custom-call | tf_op jit(solution)/shard_map/pallas_call | solution.py:361
  156.7 3.1 %shard_map.179 = (bf16[2048,512]{1,0:T(8,128)(2,1)}, bf16[2048,1024]{1,0:T(8,128)(2,1)}) custom-call(bf16[2048,256]{1,0:T(8,128)(2,1)} %get-tuple-element.32.refs_0_, bf16[256,1536]{1,0:T(8,128)(2,1)S(1)} %slice_dynamic-update-slice_fusion.refs_1_, ...), custom_call_target="tpu_custom_call", output_to_operand_aliasing={{0}: (7, {}), {1}: (8, {})} | custom-call | tf_op jit(solution)/shard_map/pallas_call | solution.py:361
  (94 shorter events, 2.1 us)
Async XLA Ops:
  0.6 0.8 copy-start
  1.5 5.6 %collective-permute-start = (bf16[128,128]{1,0:T(8,128)(2,1)S(1)}, bf16[128,128]{1,0:T(8,128)(2,1)S(1)}, u32[]{:S(2)}, u32[]{:S(2)}) collective-permute-start(bf16[128,128]{1,0:T(8,128)(2,1)S(1)} %constant_dynamic-slice_fusion), channel_id=1, source_target_pairs={{0,8},{2,10},{4,12},{6,14},{8,0},{10,2},{12,4},{14,6},{16,24},{18,... | collective-permute-start | bytes 98312 | tf_op jit(solution)/shard_map/ppermute | solution.py:21
  4.5 5.4 %collective-permute-start.1 = (bf16[128,128]{1,0:T(8,128)(2,1)S(1)}, bf16[128,128]{1,0:T(8,128)(2,1)S(1)}, u32[]{:S(2)}, u32[]{:S(2)}) collective-permute-start(bf16[128,128]{1,0:T(8,128)(2,1)S(1)} %constant_dynamic-slice_fusion), channel_id=1, source_target_pairs={{0,16},{2,18},{4,20},{6,22},{8,24},{10,26},{12,28},{14,30},{16,0},... | collective-permute-start | bytes 98312 | tf_op jit(solution)/shard_map/ppermute | solution.py:21
  7.1 5.7 %collective-permute-start.2 = (bf16[128,128]{1,0:T(8,128)(2,1)S(1)}, bf16[128,128]{1,0:T(8,128)(2,1)S(1)}, u32[]{:S(2)}, u32[]{:S(2)}) collective-permute-start(bf16[128,128]{1,0:T(8,128)(2,1)S(1)} %constant_dynamic-slice_fusion), channel_id=1, source_target_pairs={{0,24},{2,26},{4,28},{6,30},{8,16},{10,18},{12,20},{14,22},{16,8},... | collective-permute-start | bytes 98312 | tf_op jit(solution)/shard_map/ppermute | solution.py:21
  12.9 6.1 %collective-permute-start.3 = (bf16[512,128]{1,0:T(8,128)(2,1)S(1)}, bf16[512,128]{1,0:T(8,128)(2,1)S(1)}, u32[]{:S(2)}, u32[]{:S(2)}) collective-permute-start(bf16[512,128]{1,0:T(8,128)(2,1)S(1)} %pad_maximum_fusion.refs_0_), channel_id=1, source_target_pairs={{0,2},{2,0},{4,6},{6,4},{8,10},{10,8},{12,14},{14,12},{16,18},{18,... | collective-permute-start | bytes 393224 | tf_op jit(solution)/shard_map/ppermute | solution.py:21
  14.4 5.8 %collective-permute-start.4 = (bf16[512,128]{1,0:T(8,128)(2,1)S(1)}, bf16[512,128]{1,0:T(8,128)(2,1)S(1)}, u32[]{:S(2)}, u32[]{:S(2)}) collective-permute-start(bf16[512,128]{1,0:T(8,128)(2,1)S(1)} %pad_maximum_fusion.refs_0_), channel_id=1, source_target_pairs={{0,4},{2,6},{4,0},{6,2},{8,12},{10,14},{12,8},{14,10},{16,20},{18,... | collective-permute-start | bytes 393224 | tf_op jit(solution)/shard_map/ppermute | solution.py:21
  15.9 5.9 %collective-permute-start.5 = (bf16[512,128]{1,0:T(8,128)(2,1)S(1)}, bf16[512,128]{1,0:T(8,128)(2,1)S(1)}, u32[]{:S(2)}, u32[]{:S(2)}) collective-permute-start(bf16[512,128]{1,0:T(8,128)(2,1)S(1)} %pad_maximum_fusion.refs_0_), channel_id=1, source_target_pairs={{0,6},{2,4},{4,2},{6,0},{8,14},{10,12},{12,10},{14,8},{16,22},{18,... | collective-permute-start | bytes 393224 | tf_op jit(solution)/shard_map/ppermute | solution.py:21
  16.4 5.4 %collective-permute-start.6 = (bf16[512,128]{1,0:T(8,128)(2,1)S(1)}, bf16[512,128]{1,0:T(8,128)(2,1)S(1)}, u32[]{:S(2)}, u32[]{:S(2)}) collective-permute-start(bf16[512,128]{1,0:T(8,128)(2,1)S(1)} %pad_maximum_fusion.refs_0_), channel_id=1, source_target_pairs={{0,1},{1,0},{2,3},{3,2},{4,5},{5,4},{6,7},{7,6},{8,9},{9,8},{10,11... | collective-permute-start | bytes 393224 | tf_op jit(solution)/shard_map/ppermute | solution.py:102
  18.9 2.9 %collective-permute-start.7 = (bf16[512,128]{1,0:T(8,128)(2,1)S(1)}, bf16[512,128]{1,0:T(8,128)(2,1)S(1)}, u32[]{:S(2)}, u32[]{:S(2)}) collective-permute-start(bf16[512,128]{1,0:T(8,128)(2,1)S(1)} %collective-permute-done.3.refs_1_), channel_id=1, source_target_pairs={{0,1},{1,0},{2,3},{3,2},{4,5},{5,4},{6,7},{7,6},{8,9},{9,8},{10,11... | collective-permute-start | bytes 393224 | tf_op jit(solution)/shard_map/ppermute | solution.py:102
  20.2 1.6 %collective-permute-start.8 = (bf16[512,128]{1,0:T(8,128)(2,1)S(1)}, bf16[512,128]{1,0:T(8,128)(2,1)S(1)}, u32[]{:S(2)}, u32[]{:S(2)}) collective-permute-start(bf16[512,128]{1,0:T(8,128)(2,1)S(1)} %collective-permute-done.4.refs_2_), channel_id=1, source_target_pairs={{0,1},{1,0},{2,3},{3,2},{4,5},{5,4},{6,7},{7,6},{8,9},{9,8},{10,11... | collective-permute-start | bytes 393224 | tf_op jit(solution)/shard_map/ppermute | solution.py:102
  21.8 1.3 collective-permute-start.9
  29.5 8.0 %collective-permute-start.13 = (bf16[4,16,1536]{2,1,0:T(8,128)(2,1)}, bf16[4,16,1536]{2,1,0:T(8,128)(2,1)S(1)}, u32[]{:S(2)}, u32[]{:S(2)}) collective-permute-start(bf16[4,16,1536]{2,1,0:T(8,128)(2,1)} %get-tuple-element.35), channel_id=1, source_target_pairs={{0,2},{2,0},{4,6},{6,4},{8,10},{10,8},{12,14},{14,12},{16,18},{18,... | collective-permute-start | bytes 589832 | tf_op jit(solution)/shard_map/ppermute | solution.py:21
  30.1 7.4 %collective-permute-start.14 = (bf16[4,16,1536]{2,1,0:T(8,128)(2,1)}, bf16[4,16,1536]{2,1,0:T(8,128)(2,1)S(1)}, u32[]{:S(2)}, u32[]{:S(2)}) collective-permute-start(bf16[4,16,1536]{2,1,0:T(8,128)(2,1)} %get-tuple-element.36), channel_id=1, source_target_pairs={{0,4},{2,6},{4,0},{6,2},{8,12},{10,14},{12,8},{14,10},{16,20},{18,... | collective-permute-start | bytes 589832 | tf_op jit(solution)/shard_map/ppermute | solution.py:21
  30.6 10.9 %collective-permute-start.15 = (bf16[4,16,1536]{2,1,0:T(8,128)(2,1)}, bf16[4,16,1536]{2,1,0:T(8,128)(2,1)S(1)}, u32[]{:S(2)}, u32[]{:S(2)}) collective-permute-start(bf16[4,16,1536]{2,1,0:T(8,128)(2,1)} %get-tuple-element.37), channel_id=1, source_target_pairs={{0,6},{2,4},{4,2},{6,0},{8,14},{10,12},{12,10},{14,8},{16,22},{18,... | collective-permute-start | bytes 589832 | tf_op jit(solution)/shard_map/ppermute | solution.py:21
  42.6 50.2 %copy-start.7 = (f32[16,1024]{1,0:T(8,128)S(1)}, f32[16,1024]{1,0:T(8,128)}, u32[]{:S(2)}) copy-start(f32[16,1024]{1,0:T(8,128)} %first_value.1) | copy-start | bytes 196612
  42.6 50.2 %copy-start.8 = (f32[16,1024]{1,0:T(8,128)S(1)}, f32[16,1024]{1,0:T(8,128)}, u32[]{:S(2)}) copy-start(f32[16,1024]{1,0:T(8,128)} %second_value.1) | copy-start | bytes 196612
  42.7 50.9 %copy-start.9 = (f32[16,512]{1,0:T(8,128)S(1)}, f32[16,512]{1,0:T(8,128)}, u32[]{:S(2)}) copy-start(f32[16,512]{1,0:T(8,128)} %first_key.1) | copy-start | bytes 98308
  42.7 50.9 %copy-start.10 = (f32[16,512]{1,0:T(8,128)S(1)}, f32[16,512]{1,0:T(8,128)}, u32[]{:S(2)}) copy-start(f32[16,512]{1,0:T(8,128)} %second_key.1) | copy-start | bytes 98308
  42.7 4.5 %collective-permute-start.16 = (bf16[16,1536]{1,0:T(8,128)(2,1)S(1)}, bf16[16,1536]{1,0:T(8,128)(2,1)S(1)}, u32[]{:S(2)}, u32[]{:S(2)}) collective-permute-start(bf16[16,1536]{1,0:T(8,128)(2,1)S(1)} %get-tuple-element.60), channel_id=1, source_target_pairs={{0,8},{2,10},{4,12},{6,14},{8,0},{10,2},{12,4},{14,6},{16,24},{18,... | collective-permute-start | bytes 147464 | tf_op jit(solution)/shard_map/ppermute | solution.py:21
  42.8 5.7 %collective-permute-start.17 = (bf16[16,1536]{1,0:T(8,128)(2,1)S(1)}, bf16[16,1536]{1,0:T(8,128)(2,1)S(1)}, u32[]{:S(2)}, u32[]{:S(2)}) collective-permute-start(bf16[16,1536]{1,0:T(8,128)(2,1)S(1)} %get-tuple-element.62), channel_id=1, source_target_pairs={{0,16},{2,18},{4,20},{6,22},{8,24},{10,26},{12,28},{14,30},{16,0},... | collective-permute-start | bytes 147464 | tf_op jit(solution)/shard_map/ppermute | solution.py:21
  43.9 6.0 %collective-permute-start.18 = (bf16[16,1536]{1,0:T(8,128)(2,1)S(1)}, bf16[16,1536]{1,0:T(8,128)(2,1)S(1)}, u32[]{:S(2)}, u32[]{:S(2)}) collective-permute-start(bf16[16,1536]{1,0:T(8,128)(2,1)S(1)} %get-tuple-element.61), channel_id=1, source_target_pairs={{0,24},{2,26},{4,28},{6,30},{8,16},{10,18},{12,20},{14,22},{16,8},... | collective-permute-start | bytes 147464 | tf_op jit(solution)/shard_map/ppermute | solution.py:21
  49.9 4.5 %collective-permute-start.19 = (bf16[16,1536]{1,0:T(8,128)(2,1)S(1)}, bf16[16,1536]{1,0:T(8,128)(2,1)S(1)}, u32[]{:S(2)}, u32[]{:S(2)}) collective-permute-start(bf16[16,1536]{1,0:T(8,128)(2,1)S(1)} %get-tuple-element.54), channel_id=1, source_target_pairs={{0,8},{2,10},{4,12},{6,14},{8,0},{10,2},{12,4},{14,6},{16,24},{18,... | collective-permute-start | bytes 147464 | tf_op jit(solution)/shard_map/ppermute | solution.py:21
  50.7 6.4 %collective-permute-start.20 = (bf16[16,1536]{1,0:T(8,128)(2,1)S(1)}, bf16[16,1536]{1,0:T(8,128)(2,1)S(1)}, u32[]{:S(2)}, u32[]{:S(2)}) collective-permute-start(bf16[16,1536]{1,0:T(8,128)(2,1)S(1)} %get-tuple-element.54), channel_id=1, source_target_pairs={{0,16},{2,18},{4,20},{6,22},{8,24},{10,26},{12,28},{14,30},{16,0},... | collective-permute-start | bytes 147464 | tf_op jit(solution)/shard_map/ppermute | solution.py:21
  54.1 5.9 %collective-permute-start.21 = (bf16[16,1536]{1,0:T(8,128)(2,1)S(1)}, bf16[16,1536]{1,0:T(8,128)(2,1)S(1)}, u32[]{:S(2)}, u32[]{:S(2)}) collective-permute-start(bf16[16,1536]{1,0:T(8,128)(2,1)S(1)} %get-tuple-element.54), channel_id=1, source_target_pairs={{0,24},{2,26},{4,28},{6,30},{8,16},{10,18},{12,20},{14,22},{16,8},... | collective-permute-start | bytes 147464 | tf_op jit(solution)/shard_map/ppermute | solution.py:21
  60.3 6.6 %collective-permute-start.22 = (f32[16,128]{1,0:T(8,128)S(1)}, f32[16,128]{1,0:T(8,128)S(1)}, u32[]{:S(2)}, u32[]{:S(2)}) collective-permute-start(f32[16,128]{1,0:T(8,128)S(1)} %add_add_fusion.1), channel_id=1, source_target_pairs={{0,2},{2,0},{4,6},{6,4},{8,10},{10,8},{12,14},{14,12},{16,18},{18,... | collective-permute-start | bytes 24584 | tf_op jit(solution)/shard_map/ppermute | solution.py:21
  61.1 9.0 %collective-permute-start.23 = (f32[16,128]{1,0:T(8,128)S(1)}, f32[16,128]{1,0:T(8,128)S(1)}, u32[]{:S(2)}, u32[]{:S(2)}) collective-permute-start(f32[16,128]{1,0:T(8,128)S(1)} %add_add_fusion.1), channel_id=1, source_target_pairs={{0,4},{2,6},{4,0},{6,2},{8,12},{10,14},{12,8},{14,10},{16,20},{18,... | collective-permute-start | bytes 24584 | tf_op jit(solution)/shard_map/ppermute | solution.py:21
  62.4 7.8 %collective-permute-start.24 = (f32[16,128]{1,0:T(8,128)S(1)}, f32[16,128]{1,0:T(8,128)S(1)}, u32[]{:S(2)}, u32[]{:S(2)}) collective-permute-start(f32[16,128]{1,0:T(8,128)S(1)} %add_add_fusion.1), channel_id=1, source_target_pairs={{0,6},{2,4},{4,2},{6,0},{8,14},{10,12},{12,10},{14,8},{16,22},{18,... | collective-permute-start | bytes 24584 | tf_op jit(solution)/shard_map/ppermute | solution.py:21
  65.8 10.5 %collective-permute-start.10 = (bf16[16,3072]{1,0:T(8,128)(2,1)}, bf16[16,3072]{1,0:T(8,128)(2,1)S(1)}, u32[]{:S(2)}, u32[]{:S(2)}) collective-permute-start(bf16[16,3072]{1,0:T(8,128)(2,1)} %get-tuple-element.33), channel_id=1, source_target_pairs={{0,8},{2,10},{4,12},{6,14},{8,0},{10,2},{12,4},{14,6},{16,24},{18,... | collective-permute-start | bytes 294920 | tf_op jit(solution)/shard_map/ppermute | solution.py:21
  65.8 11.3 %collective-permute-start.11 = (bf16[16,3072]{1,0:T(8,128)(2,1)}, bf16[16,3072]{1,0:T(8,128)(2,1)S(1)}, u32[]{:S(2)}, u32[]{:S(2)}) collective-permute-start(bf16[16,3072]{1,0:T(8,128)(2,1)} %get-tuple-element.33), channel_id=1, source_target_pairs={{0,16},{2,18},{4,20},{6,22},{8,24},{10,26},{12,28},{14,30},{16,0},... | collective-permute-start | bytes 294920 | tf_op jit(solution)/shard_map/ppermute | solution.py:21
  66.9 10.9 %collective-permute-start.12 = (bf16[16,3072]{1,0:T(8,128)(2,1)}, bf16[16,3072]{1,0:T(8,128)(2,1)S(1)}, u32[]{:S(2)}, u32[]{:S(2)}) collective-permute-start(bf16[16,3072]{1,0:T(8,128)(2,1)} %get-tuple-element.33), channel_id=1, source_target_pairs={{0,24},{2,26},{4,28},{6,30},{8,16},{10,18},{12,20},{14,22},{16,8},... | collective-permute-start | bytes 294920 | tf_op jit(solution)/shard_map/ppermute | solution.py:21
  70.2 16.3 %collective-permute-start.32 = (bf16[128,1536]{1,0:T(8,128)(2,1)}, bf16[128,1536]{1,0:T(8,128)(2,1)S(1)}, u32[]{:S(2)}, u32[]{:S(2)}) collective-permute-start(bf16[128,1536]{1,0:T(8,128)(2,1)} %get-tuple-element.38.refs_2_), channel_id=1, source_target_pairs={{0,8},{2,10},{4,12},{6,14},{8,0},{10,2},{12,4},{14,6},{16,24},{18,... | collective-permute-start | bytes 1179656 | tf_op jit(solution)/shard_map/ppermute | solution.py:21
  70.2 20.4 %collective-permute-start.36 = (bf16[128,1536]{1,0:T(8,128)(2,1)}, bf16[128,1536]{1,0:T(8,128)(2,1)}, u32[]{:S(2)}, u32[]{:S(2)}) collective-permute-start(bf16[128,1536]{1,0:T(8,128)(2,1)} %get-tuple-element.38.refs_2_), channel_id=1, source_target_pairs={{0,16},{2,18},{4,20},{6,22},{8,24},{10,26},{12,28},{14,30},{16,0},... | collective-permute-start | bytes 1179656 | tf_op jit(solution)/shard_map/ppermute | solution.py:21
  76.3 34.0 %collective-permute-start.30 = (bf16[128,1536]{1,0:T(8,128)(2,1)}, bf16[128,1536]{1,0:T(8,128)(2,1)}, u32[]{:S(2)}, u32[]{:S(2)}) collective-permute-start(bf16[128,1536]{1,0:T(8,128)(2,1)} %get-tuple-element.38.refs_2_), channel_id=1, source_target_pairs={{0,4},{2,6},{4,0},{6,2},{8,12},{10,14},{12,8},{14,10},{16,20},{18,... | collective-permute-start | bytes 1179656 | tf_op jit(solution)/shard_map/ppermute | solution.py:21
  77.1 45.8 %collective-permute-start.29 = (bf16[128,1536]{1,0:T(8,128)(2,1)}, bf16[128,1536]{1,0:T(8,128)(2,1)}, u32[]{:S(2)}, u32[]{:S(2)}) collective-permute-start(bf16[128,1536]{1,0:T(8,128)(2,1)} %get-tuple-element.38.refs_2_), channel_id=1, source_target_pairs={{0,2},{2,0},{4,6},{6,4},{8,10},{10,8},{12,14},{14,12},{16,18},{18,... | collective-permute-start | bytes 1179656 | tf_op jit(solution)/shard_map/ppermute | solution.py:21
  77.8 12.8 %collective-permute-start.25 = (f32[16,128]{1,0:T(8,128)S(1)}, f32[16,128]{1,0:T(8,128)S(1)}, u32[]{:S(2)}, u32[]{:S(2)}) collective-permute-start(f32[16,128]{1,0:T(8,128)S(1)} %add_add_fusion), channel_id=1, source_target_pairs={{0,1},{1,0},{2,3},{3,2},{4,5},{5,4},{6,7},{7,6},{8,9},{9,8},{10,11... | collective-permute-start | bytes 24584 | tf_op jit(solution)/shard_map/ppermute | solution.py:239
  86.5 52.2 %copy-start.3 = (bf16[128,1536]{1,0:T(8,128)(2,1)}, bf16[128,1536]{1,0:T(8,128)(2,1)S(1)}, u32[]{:S(2)}) copy-start(bf16[128,1536]{1,0:T(8,128)(2,1)S(1)} %collective-permute-done.32.refs_6_) | copy-start | bytes 1179652
  86.5 37.8 %collective-permute-start.33 = (bf16[128,1536]{1,0:T(8,128)(2,1)S(1)}, bf16[128,1536]{1,0:T(8,128)(2,1)}, u32[]{:S(2)}, u32[]{:S(2)}) collective-permute-start(bf16[128,1536]{1,0:T(8,128)(2,1)S(1)} %collective-permute-done.32.refs_6_), channel_id=1, source_target_pairs={{0,2},{2,0},{4,6},{6,4},{8,10},{10,8},{12,14},{14,12},{16,18},{18,... | collective-permute-start | bytes 1179656 | tf_op jit(solution)/shard_map/ppermute | solution.py:21
  90.6 10.1 %collective-permute-start.37 = (bf16[128,1536]{1,0:T(8,128)(2,1)}, bf16[128,1536]{1,0:T(8,128)(2,1)S(1)}, u32[]{:S(2)}, u32[]{:S(2)}) collective-permute-start(bf16[128,1536]{1,0:T(8,128)(2,1)} %collective-permute-done.36.refs_2_), channel_id=1, source_target_pairs={{0,8},{2,10},{4,12},{6,14},{8,0},{10,2},{12,4},{14,6},{16,24},{18,... | collective-permute-start | bytes 1179656 | tf_op jit(solution)/shard_map/ppermute | solution.py:21
  92.1 7.8 %collective-permute-start.26 = (bf16[64,1536]{1,0:T(8,128)(2,1)S(1)}, bf16[64,1536]{1,0:T(8,128)(2,1)S(1)}, u32[]{:S(2)}, u32[]{:S(2)}) collective-permute-start(bf16[64,1536]{1,0:T(8,128)(2,1)S(1)} %fusion.1), channel_id=1, source_target_pairs={{0,2},{2,0},{4,6},{6,4},{8,10},{10,8},{12,14},{14,12},{16,18},{18,... | collective-permute-start | bytes 589832 | tf_op jit(solution)/shard_map/ppermute | solution.py:21
  99.9 9.4 %collective-permute-start.27 = (bf16[64,1536]{1,0:T(8,128)(2,1)S(1)}, bf16[64,1536]{1,0:T(8,128)(2,1)S(1)}, u32[]{:S(2)}, u32[]{:S(2)}) collective-permute-start(bf16[64,1536]{1,0:T(8,128)(2,1)S(1)} %fusion.1), channel_id=1, source_target_pairs={{0,4},{2,6},{4,0},{6,2},{8,12},{10,14},{12,8},{14,10},{16,20},{18,... | collective-permute-start | bytes 589832 | tf_op jit(solution)/shard_map/ppermute | solution.py:21
  100.7 8.8 %collective-permute-start.28 = (bf16[64,1536]{1,0:T(8,128)(2,1)S(1)}, bf16[64,1536]{1,0:T(8,128)(2,1)S(1)}, u32[]{:S(2)}, u32[]{:S(2)}) collective-permute-start(bf16[64,1536]{1,0:T(8,128)(2,1)S(1)} %fusion.1), channel_id=1, source_target_pairs={{0,6},{2,4},{4,2},{6,0},{8,14},{10,12},{12,10},{14,8},{16,22},{18,... | collective-permute-start | bytes 589832 | tf_op jit(solution)/shard_map/ppermute | solution.py:21
  109.3 12.0 %collective-permute-start.39 = (bf16[128,1536]{1,0:T(8,128)(2,1)S(1)}, bf16[128,1536]{1,0:T(8,128)(2,1)S(1)}, u32[]{:S(2)}, u32[]{:S(2)}) collective-permute-start(bf16[128,1536]{1,0:T(8,128)(2,1)S(1)} %collective-permute-done.37.refs_2_), channel_id=1, source_target_pairs={{0,4},{2,6},{4,0},{6,2},{8,12},{10,14},{12,8},{14,10},{16,20},{18,... | collective-permute-start | bytes 1179656 | tf_op jit(solution)/shard_map/ppermute | solution.py:21
  109.5 11.9 %collective-permute-start.38 = (bf16[128,1536]{1,0:T(8,128)(2,1)S(1)}, bf16[128,1536]{1,0:T(8,128)(2,1)S(1)}, u32[]{:S(2)}, u32[]{:S(2)}) collective-permute-start(bf16[128,1536]{1,0:T(8,128)(2,1)S(1)} %collective-permute-done.37.refs_2_), channel_id=1, source_target_pairs={{0,2},{2,0},{4,6},{6,4},{8,10},{10,8},{12,14},{14,12},{16,18},{18,... | collective-permute-start | bytes 1179656 | tf_op jit(solution)/shard_map/ppermute | solution.py:21
  110.3 28.3 %collective-permute-start.34 = (bf16[128,1536]{1,0:T(8,128)(2,1)S(1)}, bf16[128,1536]{1,0:T(8,128)(2,1)S(1)}, u32[]{:S(2)}, u32[]{:S(2)}) collective-permute-start(bf16[128,1536]{1,0:T(8,128)(2,1)S(1)} %collective-permute-done.32.refs_6_), channel_id=1, source_target_pairs={{0,4},{2,6},{4,0},{6,2},{8,12},{10,14},{12,8},{14,10},{16,20},{18,... | collective-permute-start | bytes 1179656 | tf_op jit(solution)/shard_map/ppermute | solution.py:21
  121.3 16.9 %collective-permute-start.43 = (bf16[128,1536]{1,0:T(8,128)(2,1)}, bf16[128,1536]{1,0:T(8,128)(2,1)S(1)}, u32[]{:S(2)}, u32[]{:S(2)}) collective-permute-start(bf16[128,1536]{1,0:T(8,128)(2,1)} %collective-permute-done.36.refs_2_), channel_id=1, source_target_pairs={{0,4},{2,6},{4,0},{6,2},{8,12},{10,14},{12,8},{14,10},{16,20},{18,... | collective-permute-start | bytes 1179656 | tf_op jit(solution)/shard_map/ppermute | solution.py:21
  121.4 18.8 %collective-permute-start.31 = (bf16[128,1536]{1,0:T(8,128)(2,1)}, bf16[128,1536]{1,0:T(8,128)(2,1)S(1)}, u32[]{:S(2)}, u32[]{:S(2)}) collective-permute-start(bf16[128,1536]{1,0:T(8,128)(2,1)} %collective-permute-done.30.refs_4_), channel_id=1, source_target_pairs={{0,2},{2,0},{4,6},{6,4},{8,10},{10,8},{12,14},{14,12},{16,18},{18,... | collective-permute-start | bytes 1179656 | tf_op jit(solution)/shard_map/ppermute | solution.py:21
  122.9 28.8 %collective-permute-start.42 = (bf16[128,1536]{1,0:T(8,128)(2,1)}, bf16[128,1536]{1,0:T(8,128)(2,1)S(1)}, u32[]{:S(2)}, u32[]{:S(2)}) collective-permute-start(bf16[128,1536]{1,0:T(8,128)(2,1)} %collective-permute-done.36.refs_2_), channel_id=1, source_target_pairs={{0,2},{2,0},{4,6},{6,4},{8,10},{10,8},{12,14},{14,12},{16,18},{18,... | collective-permute-start | bytes 1179656 | tf_op jit(solution)/shard_map/ppermute | solution.py:21
  124.2 19.9 %collective-permute-start.35 = (bf16[128,1536]{1,0:T(8,128)(2,1)}, bf16[128,1536]{1,0:T(8,128)(2,1)S(1)}, u32[]{:S(2)}, u32[]{:S(2)}) collective-permute-start(bf16[128,1536]{1,0:T(8,128)(2,1)} %collective-permute-done.33.refs_7_), channel_id=1, source_target_pairs={{0,4},{2,6},{4,0},{6,2},{8,12},{10,14},{12,8},{14,10},{16,20},{18,... | collective-permute-start | bytes 1179656 | tf_op jit(solution)/shard_map/ppermute | solution.py:21
  138.1 13.6 %copy-start.1 = (bf16[128,1536]{1,0:T(8,128)(2,1)}, bf16[128,1536]{1,0:T(8,128)(2,1)S(1)}, u32[]{:S(2)}) copy-start(bf16[128,1536]{1,0:T(8,128)(2,1)S(1)} %collective-permute-done.43.refs_4_) | copy-start | bytes 1179652
  138.1 13.5 %collective-permute-start.44 = (bf16[128,1536]{1,0:T(8,128)(2,1)S(1)}, bf16[128,1536]{1,0:T(8,128)(2,1)}, u32[]{:S(2)}, u32[]{:S(2)}) collective-permute-start(bf16[128,1536]{1,0:T(8,128)(2,1)S(1)} %collective-permute-done.43.refs_4_), channel_id=1, source_target_pairs={{0,2},{2,0},{4,6},{6,4},{8,10},{10,8},{12,14},{14,12},{16,18},{18,... | collective-permute-start | bytes 1179656 | tf_op jit(solution)/shard_map/ppermute | solution.py:21
  138.6 1.8 %copy-start.4 = (bf16[128,1536]{1,0:T(8,128)(2,1)}, bf16[128,1536]{1,0:T(8,128)(2,1)S(1)}, u32[]{:S(2)}) copy-start(bf16[128,1536]{1,0:T(8,128)(2,1)S(1)} %collective-permute-done.34.refs_8_) | copy-start | bytes 1179652
  138.6 18.1 %collective-permute-start.40 = (bf16[64,1536]{1,0:T(8,128)(2,1)}, bf16[64,1536]{1,0:T(8,128)(2,1)S(1)}, u32[]{:S(2)}, u32[]{:S(2)}) collective-permute-start(bf16[64,1536]{1,0:T(8,128)(2,1)} %slice.126), channel_id=1, source_target_pairs={{0,2},{2,0},{4,6},{6,4},{8,10},{10,8},{12,14},{14,12},{16,18},{18,... | collective-permute-start | bytes 589832 | tf_op jit(solution)/shard_map/ppermute | solution.py:21
  140.2 3.9 %copy-start.5 = (bf16[128,1536]{1,0:T(8,128)(2,1)}, bf16[128,1536]{1,0:T(8,128)(2,1)S(1)}, u32[]{:S(2)}) copy-start(bf16[128,1536]{1,0:T(8,128)(2,1)S(1)} %collective-permute-done.31.refs_5_) | copy-start | bytes 1179652
  140.2 16.5 %collective-permute-start.41 = (bf16[64,1536]{1,0:T(8,128)(2,1)S(1)}, bf16[64,1536]{1,0:T(8,128)(2,1)S(1)}, u32[]{:S(2)}, u32[]{:S(2)}) collective-permute-start(bf16[64,1536]{1,0:T(8,128)(2,1)S(1)} %slice.127), channel_id=1, source_target_pairs={{0,4},{2,6},{4,0},{6,2},{8,12},{10,14},{12,8},{14,10},{16,20},{18,... | collective-permute-start | bytes 589832 | tf_op jit(solution)/shard_map/ppermute | solution.py:21
  144.2 0.7 copy-start.6
  151.7 0.8 copy-start.2
